TPU v7x, 128 devices: a whole 4x4x4 slice. The times are simulated.
128 devices in a mesh: kv: 16 (over z, y), tp: 8 (over x, core).
Axes of the slice: x: 4, y: 4, z: 4, core: 2. Of those that a mesh axis runs over, the one named last changes fastest.
Arguments:
- hidden_rows: bfloat16 [16384, 4096], P(('kv', 'tp')), may hold values from -6 to 6
- queries: bfloat16 [16384, 4096], P('kv', 'tp'), may hold values from -6 to 6
- key_rows: bfloat16 [16384, 1024], P('kv', 'tp'), may hold values from -6 to 6
- value_rows: bfloat16 [16384, 1024], P('kv', 'tp'), may hold values from -6 to 6
- branch_gates: float32 [2, 32, 16384], P(None, 'tp', 'kv'), may hold values from 0.05 to 0.95
- log_sums: float32 [2, 32, 16384], P(None, 'tp', 'kv'), may hold values from 1 to 7
- chosen: int32 [8, 128, 16], P('tp', 'kv'), may hold values from 0 to 511, as said below
- out_grad: bfloat16 [16384, 4096], P('kv', 'tp'), may hold values from -6 to 6
Outputs:
- grad_queries: bfloat16 [16384, 4096], P('kv', 'tp')
- grad_keys: bfloat16 [16384, 1024], P('kv', 'tp')
- grad_values: bfloat16 [16384, 1024], P('kv', 'tp')
- grad_weight: float32 [4096, 4096], P('kv', 'tp')
Inputs may be any that keep to these rules, and one draw needn't show every extreme that they name: `chosen`: each list names distinct key blocks, among them the blocks that cover the query block's own rows; blocks past a query's position may be named and carry no weight for it. For one key head, the lists of the query blocks of one index of kv name at most 16 key blocks (counted with repetition) that lie at any one other index of kv.
All inputs are finite; a program needn't handle non-finite values.
Results may differ from a plain program's by a relative error of at most 0.011.
Values may be sent and summed in bfloat16 or wider, within the bound.
A program may use at most 128 MiB of HBM per device.

v0:
```python
import jax
import jax.numpy as jnp
from jax import lax
from jax.sharding import PartitionSpec as P

HEADS = 32
KV_HEADS = 8
HEAD_DIM = 128
QUERY_BLOCK = 128
KEY_BLOCK = 32
POOL_BLOCK = 32
CHOSEN = 16
CAP = 16


def sent_together(arrays, axis, dim, along):
    both = jnp.concatenate(arrays, axis=along)
    filled, at, finished = (lax.all_gather(both, axis, axis=dim, tiled=True), 0, [])
    for a in arrays:
        finished.append(lax.slice_in_dim(filled, at, at + a.shape[along], axis=along))
        at += a.shape[along]
    return tuple(finished)


def in_one_piece(arrays, axis, dim, along):
    ends, at = ([], 0)
    for a in arrays[:-1]:
        at += a.shape[along]
        ends.append(at)
    both = jnp.concatenate(arrays, axis=along)
    return tuple(
        jnp.split(lax.psum_scatter(both, axis, scatter_dimension=dim, tiled=True), ends, axis=along)
    )


def attend_back(query_rows, key_set, value_set, cotangent, log_sum, visible, score_scale):
    scores = (
        jnp.einsum("bgrd,bmd->bgrm", query_rows, key_set, preferred_element_type=jnp.float32)
        * score_scale
    )
    weights = jnp.where(visible[:, None], jnp.exp(scores - log_sum[..., None]), 0.0)
    weights_low = weights.astype(jnp.bfloat16)
    branch_out = jnp.einsum(
        "bgrm,bmd->bgrd", weights_low, value_set, preferred_element_type=jnp.float32
    )
    row_delta = jnp.sum(cotangent.astype(jnp.float32) * branch_out, axis=-1)
    grad_prob = jnp.einsum(
        "bgrd,bmd->bgrm", cotangent, value_set, preferred_element_type=jnp.float32
    )
    dscore = (weights * (grad_prob - row_delta[..., None])).astype(jnp.bfloat16)
    dquery = (
        jnp.einsum("bgrm,bmd->bgrd", dscore, key_set, preferred_element_type=jnp.float32)
        * score_scale
    )
    grad_key = (
        jnp.einsum("bgrm,bgrd->bmd", dscore, query_rows, preferred_element_type=jnp.float32)
        * score_scale
    )
    grad_value = jnp.einsum(
        "bgrm,bgrd->bmd", weights_low, cotangent, preferred_element_type=jnp.float32
    )
    return (dquery, grad_key, grad_value)


def body(hidden_rows, queries, key_rows, value_rows, branch_gates, log_sums, chosen, out_grad):
    kv_count = lax.axis_size("kv")
    kv_index = lax.axis_index("kv")
    tokens = queries.shape[0]
    kv_local = key_rows.shape[1] // HEAD_DIM
    group_size = HEADS // KV_HEADS
    score_scale = HEAD_DIM ** (-0.5)
    seq_len = tokens * kv_count
    per_device = tokens // QUERY_BLOCK
    blocks_here = tokens // KEY_BLOCK
    request_count = per_device * CHOSEN
    positions = kv_index * tokens + jnp.arange(tokens, dtype=jnp.int32)
    key_heads = key_rows.reshape(tokens, kv_local, HEAD_DIM).transpose(1, 0, 2)
    value_heads = value_rows.reshape(tokens, kv_local, HEAD_DIM).transpose(1, 0, 2)
    query_heads = queries.reshape(tokens, kv_local, group_size, HEAD_DIM).transpose(1, 2, 0, 3)
    grad_heads = (
        out_grad.reshape(tokens, kv_local, group_size, HEAD_DIM)
        .transpose(1, 2, 0, 3)
        .astype(jnp.float32)
    )
    gate_heads = branch_gates.reshape(2, kv_local, group_size, tokens)
    sum_heads = log_sums.reshape(2, kv_local, group_size, tokens)
    cot_pool = (gate_heads[0][..., None] * grad_heads).astype(jnp.bfloat16)
    cot_chosen = (gate_heads[1][..., None] * grad_heads).astype(jnp.bfloat16)
    pooled_keys = jnp.mean(
        key_heads.astype(jnp.float32).reshape(kv_local, tokens // POOL_BLOCK, POOL_BLOCK, HEAD_DIM),
        axis=2,
    ).astype(jnp.bfloat16)
    pooled_values = jnp.mean(
        value_heads.astype(jnp.float32).reshape(
            kv_local, tokens // POOL_BLOCK, POOL_BLOCK, HEAD_DIM
        ),
        axis=2,
    ).astype(jnp.bfloat16)
    every_pooled_keys, every_pooled_values = sent_together((pooled_keys, pooled_values), "kv", 1, 0)
    pool_end = jnp.arange(seq_len // POOL_BLOCK, dtype=jnp.int32) * POOL_BLOCK + POOL_BLOCK - 1
    pool_visible = (pool_end[None, :] <= positions[:, None])[None]
    pool_dquery, pool_dkeys, pool_dvalues = attend_back(
        query_heads,
        every_pooled_keys,
        every_pooled_values,
        cot_pool,
        sum_heads[0],
        pool_visible,
        score_scale,
    )
    pool_dkeys_here, pool_dvalues_here = tuple(
        (
            part.astype(jnp.float32)
            for part in in_one_piece(
                (pool_dkeys.astype(jnp.bfloat16), pool_dvalues.astype(jnp.bfloat16)), "kv", 1, 0
            )
        )
    )
    head_index = jnp.arange(kv_local, dtype=jnp.int32)[:, None]
    block_lists = chosen.reshape(kv_local, request_count)
    key_positions = (
        block_lists[..., None] * KEY_BLOCK + jnp.arange(KEY_BLOCK, dtype=jnp.int32)
    ).reshape(kv_local, per_device, CHOSEN * KEY_BLOCK)
    query_positions = positions.reshape(per_device, QUERY_BLOCK)
    chosen_visible = (key_positions[:, :, None, :] <= query_positions[None, :, :, None]).reshape(
        kv_local * per_device, QUERY_BLOCK, CHOSEN * KEY_BLOCK
    )

    def regroup(heads):
        split_rows = heads.reshape(kv_local, group_size, per_device, QUERY_BLOCK, heads.shape[-1])
        return split_rows.transpose(0, 2, 1, 3, 4).reshape(
            kv_local * per_device, group_size, QUERY_BLOCK, heads.shape[-1]
        )

    chosen_sums = regroup(sum_heads[1][..., None])[..., 0]
    owners = block_lists // blocks_here
    local_block = block_lists % blocks_here
    remote = owners != kv_index
    owner_hits = (owners[..., None] == jnp.arange(kv_count, dtype=jnp.int32)).astype(jnp.int32)
    rank_in = jnp.sum(owner_hits * (jnp.cumsum(owner_hits, axis=1) - 1), axis=-1)
    slot_count = kv_count * CAP
    slot_index = jnp.where(remote, owners * CAP + rank_in, slot_count)
    wanted = (
        jnp.zeros((kv_local, slot_count), jnp.int32)
        .at[head_index, slot_index]
        .set(local_block, mode="drop")
    )
    asked_for = lax.all_to_all(wanted, "kv", split_axis=1, concat_axis=1, tiled=True)
    key_blocks = key_heads.reshape(kv_local, blocks_here, KEY_BLOCK, HEAD_DIM)
    value_blocks = value_heads.reshape(kv_local, blocks_here, KEY_BLOCK, HEAD_DIM)
    sent_keys, sent_values = (
        lax.all_to_all(
            key_blocks[head_index, asked_for], "kv", split_axis=1, concat_axis=1, tiled=True
        ),
        lax.all_to_all(
            value_blocks[head_index, asked_for], "kv", split_axis=1, concat_axis=1, tiled=True
        ),
    )
    table_index = jnp.where(remote, blocks_here + slot_index, local_block)
    key_table = jnp.concatenate([key_blocks, sent_keys], axis=1)
    value_table = jnp.concatenate([value_blocks, sent_values], axis=1)
    dquery, grad_key, grad_value = attend_back(
        regroup(query_heads),
        key_table[head_index, table_index].reshape(
            kv_local * per_device, CHOSEN * KEY_BLOCK, HEAD_DIM
        ),
        value_table[head_index, table_index].reshape(
            kv_local * per_device, CHOSEN * KEY_BLOCK, HEAD_DIM
        ),
        regroup(cot_chosen),
        chosen_sums,
        chosen_visible,
        score_scale,
    )
    dquery = (
        dquery.reshape(kv_local, per_device, group_size, QUERY_BLOCK, HEAD_DIM)
        .transpose(0, 2, 1, 3, 4)
        .reshape(kv_local, group_size, tokens, HEAD_DIM)
    )
    pick_dquery, grad_key, grad_value = (
        dquery,
        grad_key.reshape(kv_local, request_count, KEY_BLOCK, HEAD_DIM),
        grad_value.reshape(kv_local, request_count, KEY_BLOCK, HEAD_DIM),
    )
    own_index = jnp.where(remote, blocks_here, local_block)
    pick_dkeys = (
        jnp.zeros((kv_local, blocks_here, KEY_BLOCK, HEAD_DIM), jnp.float32)
        .at[head_index, own_index]
        .add(grad_key, mode="drop")
    )
    pick_dvalues = (
        jnp.zeros((kv_local, blocks_here, KEY_BLOCK, HEAD_DIM), jnp.float32)
        .at[head_index, own_index]
        .add(grad_value, mode="drop")
    )
    back_keys = (
        jnp.zeros((kv_local, slot_count, KEY_BLOCK, HEAD_DIM), jnp.float32)
        .at[head_index, slot_index]
        .set(grad_key, mode="drop")
    )
    back_values = (
        jnp.zeros((kv_local, slot_count, KEY_BLOCK, HEAD_DIM), jnp.float32)
        .at[head_index, slot_index]
        .set(grad_value, mode="drop")
    )
    got_keys, got_values = (
        lax.all_to_all(
            back_keys.astype(jnp.bfloat16), "kv", split_axis=1, concat_axis=1, tiled=True
        ).astype(back_keys.dtype),
        lax.all_to_all(
            back_values.astype(jnp.bfloat16), "kv", split_axis=1, concat_axis=1, tiled=True
        ).astype(back_values.dtype),
    )
    owner_onehot = (
        asked_for[:, None, :] == jnp.arange(blocks_here, dtype=jnp.int32)[None, :, None]
    ).astype(jnp.float32)
    pick_dkeys = pick_dkeys + jnp.einsum(
        "kbs,ksf->kbf",
        owner_onehot,
        got_keys.reshape(kv_local, slot_count, KEY_BLOCK * HEAD_DIM),
        precision=lax.Precision.HIGHEST,
    ).reshape(kv_local, blocks_here, KEY_BLOCK, HEAD_DIM)
    pick_dvalues = pick_dvalues + jnp.einsum(
        "kbs,ksf->kbf",
        owner_onehot,
        got_values.reshape(kv_local, slot_count, KEY_BLOCK * HEAD_DIM),
        precision=lax.Precision.HIGHEST,
    ).reshape(kv_local, blocks_here, KEY_BLOCK, HEAD_DIM)
    key_total = (
        pick_dkeys.reshape(kv_local, tokens, HEAD_DIM)
        + jnp.repeat(pool_dkeys_here, POOL_BLOCK, axis=1) / POOL_BLOCK
    )
    value_total = (
        pick_dvalues.reshape(kv_local, tokens, HEAD_DIM)
        + jnp.repeat(pool_dvalues_here, POOL_BLOCK, axis=1) / POOL_BLOCK
    )
    grad_keys = (
        key_total.astype(jnp.bfloat16).transpose(1, 0, 2).reshape(tokens, kv_local * HEAD_DIM)
    )
    grad_values = (
        value_total.astype(jnp.bfloat16).transpose(1, 0, 2).reshape(tokens, kv_local * HEAD_DIM)
    )
    grad_queries = (
        (pool_dquery + pick_dquery)
        .astype(jnp.bfloat16)
        .transpose(2, 0, 1, 3)
        .reshape(tokens, kv_local * group_size * HEAD_DIM)
    )
    whole_rows = lax.all_gather(hidden_rows, "tp", axis=0, tiled=True)
    grad_weight = lax.psum_scatter(
        lax.dot_general(
            whole_rows, grad_queries, (((0,), (0,)), ((), ())), preferred_element_type=jnp.float32
        ).astype(jnp.bfloat16),
        "kv",
        scatter_dimension=0,
        tiled=True,
    ).astype(jnp.float32)
    return (grad_queries, grad_keys, grad_values, grad_weight)


def solution(mesh):
    placed = (
        P(("kv", "tp"), None),
        P("kv", "tp"),
        P("kv", "tp"),
        P("kv", "tp"),
        P(None, "tp", "kv"),
        P(None, "tp", "kv"),
        P("tp", "kv", None),
        P("kv", "tp"),
    )
    return jax.shard_map(
        body,
        mesh=mesh,
        in_specs=placed,
        out_specs=(P("kv", "tp"), P("kv", "tp"), P("kv", "tp"), P("kv", "tp")),
        check_vma=False,
    )
```

profile of v0, /device:TPU:0, one launch (start us, length us, event | category | flops | bytes accessed | tf_op | source)
XLA Modules:
  0.0 295.2 jit_solution(17730086223949128661)
XLA Ops:
  13.3 8.2 %all-to-all-start = ((s32[1,16,16]{2,0,1:T(1,128)}), s32[1,16,16]{2,0,1:T(1,128)S(1)}, u32[]{:S(2)}, u32[]{:S(2)}) async-start(s32[1,16,16]{2,0,1:T(1,128)} %all_to_all.20), calls=%async_computation | async-start | bytes 16384 | tf_op jit(solution)/shard_map/all_to_all | solution.py:148
  21.5 1.5 copy.61
  23.6 1.8 multiply_convert_fusion.3
  25.5 24.1 %all_gather.6 = bf16[2,512,128]{2,1,0:T(8,128)(2,1)S(1)} all-gather(bf16[2,32,128]{2,1,0:T(8,128)(2,1)S(1)} %pad_maximum_fusion.3), channel_id=1, replica_groups=mesh['kv'=16,'tp'=8] {'kv'}, dimensions={1}, use_global_device_ids=true | all-gather | bytes 278528 | tf_op jit(solution)/shard_map/all_gather | solution.py:18
  49.6 1.3 reshape.817
  52.2 2.2 gather_fusion
  54.5 5.1 %all-to-all-start.1 = ((bf16[1,256,32,128]{3,2,0,1:T(8,128)(2,1)}), bf16[1,256,32,128]{3,2,0,1:T(8,128)(2,1)}, u32[]{:S(2)}, u32[]{:S(2)}) async-start(bf16[1,256,32,128]{3,2,0,1:T(8,128)(2,1)} %bitcast.246), calls=%async_computation.1 | async-start | bytes 4194304 | tf_op jit(solution)/shard_map/all_to_all | solution.py:152
  60.9 2.0 fusion.7
  64.1 4.4 %multiply_convert_fusion.1 = bf16[4,1024,512]{1,2,0:T(8,128)(2,1)} fusion(f32[512,4,1024]{2,0,1:T(8,128)S(1)} %fusion.14, f32[4,1024]{1,0:T(4,128)S(1)} %fusion.7, f32[4,1024]{1,0:T(4,128)S(1)} %get-tuple-element.20, pred[1024,512]{0,1:T(8,128)(4,1)S(1)} %broadcast_compare_fusion.1, bf16[1,4,1024,128]{2,3,1,0:T(8,128)(2,1)S(1)} %copy-done.9, ...), kind=kOutput, calls=%fused_computation.12 | convolution fusion | flops 549453824 | bytes 14319616 | tf_op jit(solution)/shard_map/bgrd,bmd->bgrm/dot_general | solution.py:47
  68.5 2.3 gather_fusion.2
  70.8 15.8 %all-to-all-done.1 = bf16[1,256,32,128]{3,2,0,1:T(8,128)(2,1)} async-done(((bf16[1,256,32,128]{3,2,0,1:T(8,128)(2,1)}), bf16[1,256,32,128]{3,2,0,1:T(8,128)(2,1)}, u32[]{:S(2)}, u32[]{:S(2)}) %all-to-all-start.1) | async-done | bytes 2097184 | tf_op jit(solution)/shard_map/all_to_all | solution.py:152
  86.7 4.4 %all-to-all-start.2 = ((bf16[1,256,32,128]{3,2,0,1:T(8,128)(2,1)}), bf16[1,256,32,128]{3,2,0,1:T(8,128)(2,1)}, u32[]{:S(2)}, u32[]{:S(2)}) async-start(bf16[1,256,32,128]{3,2,0,1:T(8,128)(2,1)} %bitcast.244), calls=%async_computation.2 | async-start | bytes 4194304 | tf_op jit(solution)/shard_map/all_to_all | solution.py:155
  91.2 3.4 %fusion.12 = bf16[1,512,128]{2,1,0:T(8,128)(2,1)S(1)} fusion(bf16[4,1024,512]{1,2,0:T(8,128)(2,1)} %multiply_convert_fusion.1, bf16[1024,1,4,128]{3,2,0,1:T(4,128)(2,1)S(1)} %reshape.817), kind=kOutput, calls=%fused_computation.39 | convolution fusion | flops 537001984 | bytes 5373952 | tf_op jit(solution)/shard_map/bgrm,bgrd->bmd/dot_general | solution.py:56
  94.6 5.1 %fusion.11 = bf16[1,512,128]{2,1,0:T(8,128)(2,1)S(1)} fusion(bf16[1,4,1024,128]{2,3,1,0:T(8,128)(2,1)S(1)} %copy-done.9, f32[512,4,1024]{2,0,1:T(8,128)} %copy-done.3, f32[4,1024]{1,0:T(4,128)S(1)} %get-tuple-element.20, pred[1024,512]{0,1:T(8,128)(4,1)S(1)} %broadcast_compare_fusion.1), kind=kOutput, calls=%fused_computation.38 | convolution fusion | flops 545325056 | bytes 10108928 | tf_op jit(solution)/shard_map/bgrm,bgrd->bmd/dot_general | solution.py:59
  101.1 2.6 copy.115
  104.5 3.3 %pad_maximum_fusion = bf16[1,288,32,128]{3,2,0,1:T(8,128)(2,1)} fusion(bf16[1,256,32,128]{3,2,0,1:T(8,128)(2,1)} %all-to-all-done.1, bf16[1,32,32,128]{3,2,0,1:T(8,128)(2,1)S(1)} %bitcast.235), kind=kLoop, calls=%fused_computation.17 | loop fusion | flops 1179648 | bytes 4718592 | tf_op jit(solution)/shard_map/concatenate | solution.py:160
  107.8 2.4 gather_fusion.1
  110.2 7.7 %all-to-all-done.2 = bf16[1,256,32,128]{3,2,0,1:T(8,128)(2,1)} async-done(((bf16[1,256,32,128]{3,2,0,1:T(8,128)(2,1)}), bf16[1,256,32,128]{3,2,0,1:T(8,128)(2,1)}, u32[]{:S(2)}, u32[]{:S(2)}) %all-to-all-start.2) | async-done | bytes 2097184 | tf_op jit(solution)/shard_map/all_to_all | solution.py:155
  117.9 3.3 %pad_maximum_fusion.1 = bf16[1,288,32,128]{3,2,0,1:T(8,128)(2,1)} fusion(bf16[1,256,32,128]{3,2,0,1:T(8,128)(2,1)} %all-to-all-done.2, bf16[1,32,32,128]{3,2,0,1:T(8,128)(2,1)S(1)} %bitcast.237), kind=kLoop, calls=%fused_computation.18 | loop fusion | flops 1179648 | bytes 4718592 | tf_op jit(solution)/shard_map/concatenate | solution.py:161
  121.2 3.3 %gather_fusion.3 = bf16[128,32,128]{2,1,0:T(8,128)(2,1)} fusion(bf16[1,288,32,128]{3,2,0,1:T(8,128)(2,1)} %pad_maximum_fusion.1, s32[128]{0:T(128)S(1)} %or_bitcast_fusion), kind=kCustom, calls=%fused_computation.3 | custom fusion | bytes 2098176 | tf_op jit(solution)/shard_map/gather | solution.py:167
  126.1 2.0 multiply_reduce_fusion
  129.0 2.9 multiply_convert_fusion
  131.9 2.0 copy-done.4
  133.9 2.9 multiply_bitcast_fusion
  136.7 2.9 copy.76
  139.6 1.9 reshape.829
  141.6 4.6 %add_convert_fusion = bf16[4,1024,128]{1,2,0:T(8,128)(2,1)} fusion(f32[4,1024,128]{1,2,0:T(8,128)S(1)} %reshape.829, bf16[4,1024,512]{1,2,0:T(8,128)(2,1)} %multiply_convert_fusion.1, bf16[2,512,128]{2,1,0:T(8,128)(2,1)S(1)} %all_gather.6), kind=kOutput, calls=%fused_computation.28 | convolution fusion | flops 538443776 | bytes 7471104 | tf_op jit(solution)/shard_map/bgrm,bmd->bgrd/dot_general | solution.py:52
  146.2 10.2 %fusion.2 = bf16[4096,512]{0,1:T(8,128)(2,1)} fusion(bf16[1024,512]{0,1:T(8,128)(2,1)} %bitcast.247, bf16[1024,4096]{1,0:T(8,128)(2,1)} %all-gather.2.cloned.1.call-done), kind=kOutput, calls=%fused_computation.16 | convolution fusion | flops 4297064448 | bytes 13631488 | tf_op jit(solution)/shard_map/dot_general | solution.py:251
  156.4 3.7 %bitcast_multiply_fusion = f32[8,512,128]{2,1,0:T(8,128)S(1)} fusion(bf16[8,4,128,512]{2,3,1,0:T(8,128)(2,1)} %copy-done.4, bf16[1,4,8,128,128]{4,3,2,1,0:T(8,128)(2,1)} %bitcast.250), kind=kOutput, calls=%fused_computation.23 | convolution fusion | flops 537395200 | bytes 7340032 | tf_op jit(solution)/shard_map/bgrm,bgrd->bmd/dot_general | solution.py:56
  160.2 2.5 broadcast.720.clone.1
  162.6 15.8 %scatter_fusion = f32[256,32,128]{2,1,0:T(8,128)} fusion(f32[256,32,128]{2,1,0:T(8,128)} %broadcast.720.clone.1, s32[128]{0:T(128)S(1)} %fusion.38, f32[128,32,128]{2,1,0:T(8,128)S(1)} %bitcast.240), kind=kCustom, calls=%fused_computation.5 | custom fusion | bytes 6291968 | tf_op jit(solution)/shard_map/scatter | solution.py:199
  178.4 4.0 %convert_bitcast_fusion.1 = bf16[1,256,32,128]{3,2,0,1:T(8,128)(2,1)} fusion(f32[256,32,128]{2,1,0:T(8,128)} %scatter_fusion), kind=kLoop, calls=%fused_computation.27 | loop fusion | flops 1048576 | bytes 6291456 | tf_op jit(solution)/shard_map/convert_element_type | solution.py:208
  182.4 4.4 %all-to-all-start.3 = ((bf16[1,256,32,128]{3,2,0,1:T(8,128)(2,1)}), bf16[1,256,32,128]{3,2,0,1:T(8,128)(2,1)}, u32[]{:S(2)}, u32[]{:S(2)}) async-start(bf16[1,256,32,128]{3,2,0,1:T(8,128)(2,1)} %convert_bitcast_fusion.1), calls=%async_computation.3 | async-start | bytes 4194304 | tf_op jit(solution)/shard_map/all_to_all | solution.py:207
  186.8 6.7 %fusion.21 = f32[8,512,128,1]{2,1,3,0:T(8,128)} fusion(bf16[8,4,128,128]{2,0,3,1:T(8,128)(2,1)} %bitcast.252, f32[8,512,4,128]{3,1,2,0:T(8,128)} %copy-done.2, f32[8,4,128]{2,1,0:T(4,128)S(1)} %get-tuple-element.21, pred[8,128,512]{1,2,0:T(8,128)(4,1)S(1)} %broadcast_compare_fusion), kind=kOutput, calls=%fused_computation.51 | convolution fusion | flops 545259520 | bytes 12075008 | tf_op jit(solution)/shard_map/bgrm,bgrd->bmd/dot_general | solution.py:59
  193.5 2.5 broadcast.720.clone
  196.0 17.6 %scatter_fusion.2 = f32[256,32,128]{2,1,0:T(8,128)} fusion(f32[256,32,128]{2,1,0:T(8,128)} %broadcast.720.clone, s32[128]{0:T(128)S(1)} %fusion.38, f32[128,32,128]{2,1,0:T(8,128)} %bitcast.242), kind=kCustom, calls=%fused_computation.7 | custom fusion | bytes 6291968 | tf_op jit(solution)/shard_map/scatter | solution.py:204
  213.5 4.1 %convert_bitcast_fusion = bf16[1,256,32,128]{3,2,0,1:T(8,128)(2,1)} fusion(f32[256,32,128]{2,1,0:T(8,128)} %scatter_fusion.2), kind=kLoop, calls=%fused_computation.26 | loop fusion | flops 1048576 | bytes 6291456 | tf_op jit(solution)/shard_map/convert_element_type | solution.py:211
  217.7 7.3 %all-to-all-start.4 = ((bf16[1,256,32,128]{3,2,0,1:T(8,128)(2,1)}), bf16[1,256,32,128]{3,2,0,1:T(8,128)(2,1)}, u32[]{:S(2)}, u32[]{:S(2)}) async-start(bf16[1,256,32,128]{3,2,0,1:T(8,128)(2,1)} %convert_bitcast_fusion), calls=%async_computation.5 | async-start | bytes 4194304 | tf_op jit(solution)/shard_map/all_to_all | solution.py:210
  225.8 2.3 copy.85
  228.1 4.3 %copy.110 = bf16[1,256,32,128]{1,3,2,0:T(8,128)(2,1)} copy(bf16[1,256,32,128]{3,2,0,1:T(8,128)(2,1)} %all-to-all-done.3) | data formatting | bytes 4194304 | tf_op jit(solution)/shard_map/reshape.64
  232.4 2.3 fusion.5
  235.0 19.9 %all-to-all-done.4 = bf16[1,256,32,128]{3,2,0,1:T(8,128)(2,1)} async-done(((bf16[1,256,32,128]{3,2,0,1:T(8,128)(2,1)}), bf16[1,256,32,128]{3,2,0,1:T(8,128)(2,1)}, u32[]{:S(2)}, u32[]{:S(2)}) %all-to-all-start.4) | async-done | bytes 2097184 | tf_op jit(solution)/shard_map/all_to_all | solution.py:210
  254.9 4.3 %copy.113 = bf16[1,256,32,128]{1,3,2,0:T(8,128)(2,1)} copy(bf16[1,256,32,128]{3,2,0,1:T(8,128)(2,1)} %all-to-all-done.4) | data formatting | bytes 4194304 | tf_op jit(solution)/shard_map/reshape.75
  259.2 2.3 fusion.3
  261.8 5.9 %scatter_fusion.1 = f32[32,32,128]{2,1,0:T(8,128)S(1)} fusion(f32[32,32,128]{2,1,0:T(8,128)S(1)} %copy.79, s32[128]{0:T(128)S(1)} %fusion.39, f32[128,32,128]{2,1,0:T(8,128)S(1)} %bitcast.241), kind=kCustom, calls=%fused_computation.6 | custom fusion | flops 524288 | bytes 6291968 | tf_op jit(solution)/shard_map/scatter-add | solution.py:189
  267.7 11.9 %scatter_fusion.3 = f32[32,32,128]{2,1,0:T(8,128)S(1)} fusion(f32[32,32,128]{2,1,0:T(8,128)S(1)} %copy.84, s32[128]{0:T(128)S(1)} %fusion.39, f32[128,32,128]{2,1,0:T(8,128)} %bitcast.243), kind=kCustom, calls=%fused_computation.8 | custom fusion | flops 524288 | bytes 6291968 | tf_op jit(solution)/shard_map/scatter-add | solution.py:194
  280.5 5.4 %reduce-scatter.5.cloned.1.call-done = bf16[256,512]{0,1:T(8,128)(2,1)} async-done(((bf16[4096,512]{0,1:T(8,128)(2,1)}), bf16[256,512]{0,1:T(8,128)(2,1)}) %reduce-scatter.5.cloned.1.call-update) | async-done | bytes 262160 | tf_op jit(solution)/shard_map/reduce_scatter | solution.py:250
  285.9 1.9 copy.86
  (83 shorter events, 16.5 us)
Async XLA Ops:
  8.0 15.0 %copy-start = (bf16[1024,128]{1,0:T(8,128)(2,1)S(1)}, bf16[1024,128]{1,0:T(8,128)(2,1)}, u32[]{:S(2)}) copy-start(bf16[1024,128]{1,0:T(8,128)(2,1)} %param.10) | copy-start | bytes 786436
  8.0 15.1 %copy-start.1 = (bf16[1024,128]{1,0:T(8,128)(2,1)S(1)}, bf16[1024,128]{1,0:T(8,128)(2,1)}, u32[]{:S(2)}) copy-start(bf16[1024,128]{1,0:T(8,128)(2,1)} %param.11) | copy-start | bytes 786436
  8.0 15.2 %copy-start.10 = (f32[2,4,1024]{2,1,0:T(4,128)S(1)}, f32[2,4,1024]{2,1,0:T(4,128)}, u32[]{:S(2)}) copy-start(f32[2,4,1024]{2,1,0:T(4,128)} %param.13) | copy-start | bytes 98308
  8.0 15.2 %copy-start.11 = (f32[2,4,1024]{2,1,0:T(4,128)S(1)}, f32[2,4,1024]{2,1,0:T(4,128)}, u32[]{:S(2)}) copy-start(f32[2,4,1024]{2,1,0:T(4,128)} %param.12) | copy-start | bytes 98308
  8.0 138.2 %all-gather.2.cloned.1.call-start = ((), (), s32[]{:S(2)}) async-start(), calls=%async_computation.8 | async-start | bytes 9437184 | tf_op jit(solution)/shard_map/all_gather | solution.py:249
  13.3 37.6 %all-to-all-start = ((s32[1,16,16]{2,0,1:T(1,128)}), s32[1,16,16]{2,0,1:T(1,128)S(1)}, u32[]{:S(2)}, u32[]{:S(2)}) async-start(s32[1,16,16]{2,0,1:T(1,128)} %all_to_all.20), calls=%async_computation | async-start | bytes 16384 | tf_op jit(solution)/shard_map/all_to_all | solution.py:148
  54.5 32.2 %all-to-all-start.1 = ((bf16[1,256,32,128]{3,2,0,1:T(8,128)(2,1)}), bf16[1,256,32,128]{3,2,0,1:T(8,128)(2,1)}, u32[]{:S(2)}, u32[]{:S(2)}) async-start(bf16[1,256,32,128]{3,2,0,1:T(8,128)(2,1)} %bitcast.246), calls=%async_computation.1 | async-start | bytes 4194304 | tf_op jit(solution)/shard_map/all_to_all | solution.py:152
  59.6 1.3 copy-start.9
  60.9 3.2 %copy-start.3 = (f32[512,4,1024]{2,0,1:T(8,128)}, f32[512,4,1024]{2,0,1:T(8,128)S(1)}, u32[]{:S(2)}) copy-start(f32[512,4,1024]{2,0,1:T(8,128)S(1)} %fusion.14) | copy-start | bytes 25165828
  86.7 31.2 %all-to-all-start.2 = ((bf16[1,256,32,128]{3,2,0,1:T(8,128)(2,1)}), bf16[1,256,32,128]{3,2,0,1:T(8,128)(2,1)}, u32[]{:S(2)}, u32[]{:S(2)}) async-start(bf16[1,256,32,128]{3,2,0,1:T(8,128)(2,1)} %bitcast.244), calls=%async_computation.2 | async-start | bytes 4194304 | tf_op jit(solution)/shard_map/all_to_all | solution.py:155
  91.1 134.0 %reduce-scatter.3.cloned.1.call-start = ((), (), s32[]{:S(2)}) async-start(), calls=%async_computation.7 | async-start | bytes 278528 | tf_op jit(solution)/shard_map/reduce_scatter | solution.py:32
  100.5 185.4 %reduce-scatter.5.cloned.1.call-start = ((), (), s32[]{:S(2)}) async-start(), calls=%async_computation.9 | async-start | bytes 4456448 | tf_op jit(solution)/shard_map/reduce_scatter | solution.py:250
  100.8 23.7 %copy-start.5 = (bf16[1024,1,4,128]{3,0,2,1:T(8,128)(2,1)}, bf16[1024,1,4,128]{3,0,2,1:T(8,128)(2,1)S(1)}, u32[]{:S(2)}) copy-start(bf16[1024,1,4,128]{3,0,2,1:T(8,128)(2,1)S(1)} %copy.60) | copy-start | bytes 3145732
  124.5 1.3 copy-start.6
  124.5 1.5 copy-start.8
  125.8 3.2 %copy-start.2 = (f32[8,512,4,128]{3,1,2,0:T(8,128)}, f32[8,512,4,128]{3,1,2,0:T(8,128)S(1)}, u32[]{:S(2)}) copy-start(f32[8,512,4,128]{3,1,2,0:T(8,128)S(1)} %fusion.17) | copy-start | bytes 25165828
  126.1 2.9 copy-start.7
  131.9 2.0 copy-start.4
  182.4 35.3 %all-to-all-start.3 = ((bf16[1,256,32,128]{3,2,0,1:T(8,128)(2,1)}), bf16[1,256,32,128]{3,2,0,1:T(8,128)(2,1)}, u32[]{:S(2)}, u32[]{:S(2)}) async-start(bf16[1,256,32,128]{3,2,0,1:T(8,128)(2,1)} %convert_bitcast_fusion.1), calls=%async_computation.3 | async-start | bytes 4194304 | tf_op jit(solution)/shard_map/all_to_all | solution.py:207
  217.7 37.3 %all-to-all-start.4 = ((bf16[1,256,32,128]{3,2,0,1:T(8,128)(2,1)}), bf16[1,256,32,128]{3,2,0,1:T(8,128)(2,1)}, u32[]{:S(2)}, u32[]{:S(2)}) async-start(bf16[1,256,32,128]{3,2,0,1:T(8,128)(2,1)} %convert_bitcast_fusion), calls=%async_computation.5 | async-start | bytes 4194304 | tf_op jit(solution)/shard_map/all_to_all | solution.py:210
Sparse Core Ops, SparseCore 0:
  10.6 52.0 all-gather.1
Sparse Core Ops, SparseCore 1:
  100.5 74.6 reduce-scatter.2
  178.4 107.5 reduce-scatter.4
where the time goes:
time: 298 us; the launch traced here: 295 us
  local copies, waits for them, and re-layouts  81.8 us (27%)
  matrix products  55 us (18%)
  waiting for transfers between devices  49.5 us (17%)
  other arithmetic  39 us (13%)
  starting transfers between devices  29.8 us (10%)
  blocking collectives  24.1 us (8%)
  between operations  16 us (5%)
    all_gather x1, blocking collectives, sent_together(): lax.all_gather(both, axis, axis=dim, tiled=True)  24.1 us
    all_to_all x1, waiting for transfers between devices, body(): lax.all_to_all(back_values.astype(jnp.bfloat16), 'kv', split_axis=1, conc...  19.9 us
    scatter x1, local copies, waits for them, and re-layouts, body(): back_values = jnp.zeros((kv_local, slot_count, KEY_BLOCK, HEAD_DIM), jnp....  17.6 us
    all_to_all x1, waiting for transfers between devices, body(): lax.all_to_all(key_blocks[head_index, asked_for], 'kv', split_axis=1, con...  15.8 us
    scatter x1, local copies, waits for them, and re-layouts, body(): back_keys = jnp.zeros((kv_local, slot_count, KEY_BLOCK, HEAD_DIM), jnp.fl...  15.8 us
    another operation x4, local copies, waits for them, and re-layouts  13.5 us
    scatter-add x1, other arithmetic, body(): pick_dvalues = jnp.zeros((kv_local, blocks_here, KEY_BLOCK, HEAD_DIM), jn...  11.9 us
    dot_general x2, matrix products, attend_back(): jnp.einsum('bgrm,bgrd->bmd', weights_low, cotangent, preferred_element_ty...  11.7 us
  transfers between devices with their start and end apart: 8, of which 4 were waited for; matrix products, arithmetic and copies ran while one was open for 57% of the time, Pallas kernels for 0%

commit v1 on v0

v1 whole, which is shorter than its diff:
```python
import jax
import jax.numpy as jnp
from jax import lax
from jax.experimental import pallas as pl
from jax.experimental.pallas import tpu as pltpu
from jax.sharding import PartitionSpec as P

HEADS = 32
KV_HEADS = 8
HEAD_DIM = 128
QUERY_BLOCK = 128
KEY_BLOCK = 32
POOL_BLOCK = 32
CHOSEN = 16
GROUP = HEADS // KV_HEADS
SIDE = 4
OWNERS = SIDE * SIDE
TOKENS = 1024
BLOCKS = TOKENS // QUERY_BLOCK
POOLED = TOKENS // POOL_BLOCK
SEQ = TOKENS * OWNERS
MODEL = 4096
SCALE = HEAD_DIM ** (-0.5)
LOG2E = 1.4426950408889634
MESH = pl.DeviceIdType.MESH
F32 = jnp.float32
BF16 = jnp.bfloat16

NT = (((1,), (1,)), ((), ()))
NN = (((1,), (0,)), ((), ()))


def dot(a, b, dims):
    return lax.dot_general(a, b, dims, preferred_element_type=F32)


class Sender:
    def __init__(self, send_sems, recv_sems):
        self.send_sems, self.recv_sems, self.at, self.sent = send_sems, recv_sems, 0, []

    def __call__(self, src, dst, dev):
        copy = pltpu.make_async_remote_copy(
            src_ref=src,
            dst_ref=dst,
            send_sem=self.send_sems.at[self.at],
            recv_sem=self.recv_sems.at[self.at],
            device_id=dev,
            device_id_type=MESH,
        )
        self.at += 1
        copy.start()
        self.sent.append(copy)
        return copy

    def finish(self):
        for copy in self.sent:
            copy.wait_send()


def place():
    kv, tp = lax.axis_index("kv"), lax.axis_index("tp")
    return kv, tp, kv // SIDE, kv % SIDE, tp // 2, tp % 2


def shifted(c, o):
    return (c + (o + SIDE)) % SIDE


def meet(devices):
    barrier = pltpu.get_barrier_semaphore()
    for dev in devices:
        pl.semaphore_signal(barrier, inc=1, device_id=dev, device_id_type=MESH)
    pl.semaphore_wait(barrier, len(devices))


def tile_operands(q_ref, g_ref, gate_ref, ls_ref, branch, t):
    rows = pl.ds(pl.multiple_of(t * QUERY_BLOCK, QUERY_BLOCK), QUERY_BLOCK)
    gates = jnp.concatenate([gate_ref[0, :, rows], gate_ref[1, :, rows]], axis=0).T
    qs, cs, ls = [], [], []
    for h in range(GROUP):
        cols = slice(h * HEAD_DIM, (h + 1) * HEAD_DIM)
        qs.append(q_ref[rows, cols])
        at = branch * GROUP + h
        cs.append((gates[:, at : at + 1] * g_ref[rows, cols].astype(F32)).astype(BF16))
        ls.append(ls_ref[branch, h : h + 1, rows])
    return (
        jnp.concatenate(qs, axis=0),
        jnp.concatenate(cs, axis=0),
        jnp.concatenate(ls, axis=1) * LOG2E,
    )


def attend_back(qs, cs, log_sum, keys, values, visible):
    scores = dot(keys, qs, NT) * (SCALE * LOG2E)
    p = jnp.where(visible, jnp.exp2(scores - log_sum), 0.0)
    pr = p.astype(BF16)
    dp = dot(values, cs, NT)
    delta = jnp.sum(pr.astype(F32) * dp, axis=0, keepdims=True)
    ds = (p * (dp - delta)).astype(BF16)
    return dot(keys.T, ds, NN), dot(ds, qs, NN), dot(pr, cs, NN)


def gather_kernel(
    k_ref, v_ref, h_ref, q_ref, g_ref, gate_ref, ls_ref,
    k_all, v_all, h_all, dq_ref, dpk_ref, dpv_ref,
    pool_all, pk_ref, pv_ref, pool_here,
    pool_send, pool_recv, send_sems, recv_sems, local_sems,
):
    kv, tp, cz, cy, cx, core = place()
    half = TOKENS // 2

    def device(oz, oy):
        return (shifted(cz, oz) * SIDE + shifted(cy, oy), tp)

    def along(axis, o):
        return device(o, 0) if axis == 0 else device(0, o)

    def owner(axis, o1, o2):
        a, b = (o1, o2) if axis == 0 else (o2, o1)
        return shifted(cz, a) * SIDE + shifted(cy, b)

    def xdev(o, c):
        return (kv, shifted(cx, o) * 2 + c)

    local = [
        pltpu.make_async_copy(k_ref, k_all.at[kv], local_sems.at[0]),
        pltpu.make_async_copy(v_ref, v_all.at[kv], local_sems.at[1]),
        pltpu.make_async_copy(h_ref, h_all.at[tp], local_sems.at[2]),
    ]
    for copy in local:
        copy.start()

    blk = lax.broadcasted_iota(jnp.int32, (POOLED, TOKENS), 0)
    row = lax.broadcasted_iota(jnp.int32, (POOLED, TOKENS), 1)
    mean = jnp.where(row // POOL_BLOCK == blk, 1.0 / POOL_BLOCK, 0.0).astype(BF16)
    pool_here[0] = dot(mean, k_ref[...], NN).astype(BF16)
    pool_here[1] = dot(mean, v_ref[...], NN).astype(BF16)

    others = [(oz, oy) for oz in range(SIDE) for oy in range(SIDE) if (oz, oy) != (0, 0)]
    meet([device(oz, oy) for oz, oy in others] + [xdev(1, core), xdev(-1, core), xdev(0, 1 - core)])

    pool_sender = Sender(pool_send, pool_recv)
    for oz, oy in others:
        pool_sender(pool_here, pool_all.at[kv], device(oz, oy))
    pool_all[kv] = pool_here[...]

    send = Sender(send_sems, recv_sems)
    first, wide = {}, {}
    arrays = ((0, k_ref, k_all), (1, v_ref, v_all))
    for axis, here, full in arrays:
        first[axis] = [send(here, full.at[kv], along(axis, s)) for s in (1, -1)]
    x_first = [send(h_ref, h_all.at[tp], xdev(s, core)) for s in (1, -1)]
    x_over = [send(h_ref, h_all.at[tp], xdev(0, 1 - core))]
    for axis, here, full in arrays:
        wide[axis] = [(0, [send(here, full.at[kv], along(1 - axis, s)) for s in (1, -1)])]

    for copy in pool_sender.sent:
        copy.wait_recv()
    pk_ref[...] = pool_all[:, 0].reshape(OWNERS * POOLED, HEAD_DIM)
    pv_ref[...] = pool_all[:, 1].reshape(OWNERS * POOLED, HEAD_DIM)
    dpk_ref[...] = jnp.zeros_like(dpk_ref)
    dpv_ref[...] = jnp.zeros_like(dpv_ref)

    n_pool = OWNERS * POOLED
    wide_q = GROUP * QUERY_BLOCK
    pool_end = lax.broadcasted_iota(jnp.int32, (n_pool, wide_q), 0) * POOL_BLOCK + POOL_BLOCK - 1
    lane = lax.broadcasted_iota(jnp.int32, (n_pool, wide_q), 1) % QUERY_BLOCK
    ahead = pool_end - lane

    def tile(t, carry):
        qs, cs, log_sum = tile_operands(q_ref, g_ref, gate_ref, ls_ref, 0, t)
        visible = ahead <= kv * TOKENS + t * QUERY_BLOCK
        dq, dk, dv = attend_back(qs, cs, log_sum, pk_ref[...], pv_ref[...], visible)
        dq_ref[t] = dq
        dpk_ref[...] += dk
        dpv_ref[...] += dv
        return carry

    lax.fori_loop(0, 4, tile, 0)

    second = {}
    for axis, here, full in arrays:
        plus, minus = first[axis]
        plus.wait_recv()
        part = full.at[owner(axis, -1, 0), pl.ds(0, half)]
        fwd = send(part, part, along(axis, 1))
        whole = full.at[owner(axis, -1, 0)]
        wide[axis].append((-1, [send(whole, whole, along(1 - axis, s)) for s in (1, -1)]))
        minus.wait_recv()
        part = full.at[owner(axis, 1, 0), pl.ds(half, half)]
        bwd = send(part, part, along(axis, -1))
        whole = full.at[owner(axis, 1, 0)]
        wide[axis].append((1, [send(whole, whole, along(1 - axis, s)) for s in (1, -1)]))
        second[axis] = (fwd, bwd)

    lax.fori_loop(4, BLOCKS, tile, 0)
    dpk_ref[...] = dpk_ref[...] * SCALE

    last = []

    def across(axis, full, o, pair):
        plus, minus = pair
        plus.wait_recv()
        part = full.at[owner(axis, o, -1), pl.ds(0, half)]
        last.append(send(part, part, along(1 - axis, 1)))
        minus.wait_recv()
        part = full.at[owner(axis, o, 1), pl.ds(half, half)]
        last.append(send(part, part, along(1 - axis, -1)))

    for axis, here, full in arrays:
        across(axis, full, *wide[axis][0])
    for axis, here, full in arrays:
        for copy in second[axis]:
            copy.wait_recv()
        whole = full.at[owner(axis, 2, 0)]
        wide[axis].append((2, [send(whole, whole, along(1 - axis, s)) for s in (1, -1)]))
    rows = h_ref.shape[0] // 2
    plus, minus = x_first
    plus.wait_recv()
    whole = h_all.at[shifted(cx, -1) * 2 + core]
    part = whole.at[pl.ds(0, rows)]
    x_second = [send(part, part, xdev(1, core))]
    x_over.append(send(whole, whole, xdev(0, 1 - core)))
    minus.wait_recv()
    whole = h_all.at[shifted(cx, 1) * 2 + core]
    part = whole.at[pl.ds(rows, rows)]
    x_second.append(send(part, part, xdev(-1, core)))
    x_over.append(send(whole, whole, xdev(0, 1 - core)))
    for i in (1, 2):
        for axis, here, full in arrays:
            across(axis, full, *wide[axis][i])
    for copy in x_second:
        copy.wait_recv()
    whole = h_all.at[shifted(cx, 2) * 2 + core]
    x_over.append(send(whole, whole, xdev(0, 1 - core)))
    for axis, here, full in arrays:
        across(axis, full, *wide[axis][3])
    for copy in last:
        copy.wait_recv()
    for copy in x_over:
        copy.wait_recv()
    pool_sender.finish()
    send.finish()
    for copy in local:
        copy.wait()


GATHER_COPIES = 2 * (2 + 2 + 8 + 8) + 2 + 2 + 4


def run_gather(k, v, h, q, g, gates, sums):
    any_spec = pl.BlockSpec(memory_space=pl.ANY)
    vmem = pl.BlockSpec(memory_space=pltpu.VMEM)
    n_pool = OWNERS * POOLED
    return pl.pallas_call(
        gather_kernel,
        name="gather",
        out_shape=(
            jax.ShapeDtypeStruct((OWNERS, TOKENS, HEAD_DIM), BF16),
            jax.ShapeDtypeStruct((OWNERS, TOKENS, HEAD_DIM), BF16),
            jax.ShapeDtypeStruct((8, TOKENS // 8, MODEL), BF16),
            jax.ShapeDtypeStruct((BLOCKS, HEAD_DIM, GROUP * QUERY_BLOCK), F32),
            jax.ShapeDtypeStruct((n_pool, HEAD_DIM), F32),
            jax.ShapeDtypeStruct((n_pool, HEAD_DIM), F32),
        ),
        in_specs=[vmem] * 7,
        out_specs=(any_spec, any_spec, any_spec, vmem, vmem, vmem),
        scratch_shapes=[
            pltpu.VMEM((OWNERS, 2, POOLED, HEAD_DIM), BF16),
            pltpu.VMEM((n_pool, HEAD_DIM), BF16),
            pltpu.VMEM((n_pool, HEAD_DIM), BF16),
            pltpu.VMEM((2, POOLED, HEAD_DIM), BF16),
            pltpu.SemaphoreType.DMA((OWNERS - 1,)),
            pltpu.SemaphoreType.DMA((OWNERS - 1,)),
            pltpu.SemaphoreType.DMA((GATHER_COPIES,)),
            pltpu.SemaphoreType.DMA((GATHER_COPIES,)),
            pltpu.SemaphoreType.DMA((3,)),
        ],
        compiler_params=pltpu.CompilerParams(collective_id=0, has_side_effects=True),
    )(k, v, h, q, g, gates, sums)


def chosen_kernel(
    chosen_ref, k_ref, v_ref, q_ref, g_ref, gate_ref, ls_ref, dqp_ref, dpk_ref, dpv_ref,
    gq_ref, gqt_ref, dk_ref, dv_ref,
    acc_k, acc_v, kb, vb,
):
    kv = lax.axis_index("kv")
    n_pool = OWNERS * POOLED

    def start(i, carry):
        at = pl.multiple_of(i * 8, 8)
        for acc, pooled in ((acc_k, dpk_ref), (acc_v, dpv_ref)):
            part = pooled[pl.ds(at, 8), :] * (1.0 / POOL_BLOCK)
            rows = jnp.broadcast_to(part[:, None, :], (8, POOL_BLOCK, HEAD_DIM))
            acc[pl.ds(pl.multiple_of(at * POOL_BLOCK, 8 * POOL_BLOCK), 8 * POOL_BLOCK), :] = (
                rows.reshape(8 * POOL_BLOCK, HEAD_DIM)
            )
        return carry

    lax.fori_loop(0, n_pool // 8, start, 0)

    wide_q = GROUP * QUERY_BLOCK
    ahead = (
        lax.broadcasted_iota(jnp.int32, (KEY_BLOCK, wide_q), 0)
        - lax.broadcasted_iota(jnp.int32, (KEY_BLOCK, wide_q), 1) % QUERY_BLOCK
    )

    def block(b, carry):
        qs, cs, log_sum = tile_operands(q_ref, g_ref, gate_ref, ls_ref, 1, b)
        start_row = kv * TOKENS + b * QUERY_BLOCK
        seen, at = [], []
        for c in range(CHOSEN):
            first = pl.multiple_of(chosen_ref[b, c] * KEY_BLOCK, KEY_BLOCK)
            at.append(first)
            kb[pl.ds(c * KEY_BLOCK, KEY_BLOCK), :] = k_ref[pl.ds(first, KEY_BLOCK), :]
            vb[pl.ds(c * KEY_BLOCK, KEY_BLOCK), :] = v_ref[pl.ds(first, KEY_BLOCK), :]
            seen.append(ahead <= start_row - first)
        visible = jnp.concatenate(seen, axis=0)
        dq, dk, dv = attend_back(qs, cs, log_sum, kb[...], vb[...], visible)
        dk = dk * SCALE
        total = (dqp_ref[b] + dq) * SCALE
        rows = pl.ds(pl.multiple_of(b * QUERY_BLOCK, QUERY_BLOCK), QUERY_BLOCK)
        for h in range(GROUP):
            cols = slice(h * HEAD_DIM, (h + 1) * HEAD_DIM)
            part = total[:, cols]
            gqt_ref[cols, rows] = part.astype(BF16)
            gq_ref[rows, cols] = part.T.astype(BF16)
        for c in range(CHOSEN):
            here = pl.ds(at[c], KEY_BLOCK)
            piece = slice(c * KEY_BLOCK, (c + 1) * KEY_BLOCK)
            acc_k[here, :] += dk[piece]
            acc_v[here, :] += dv[piece]
        return carry

    lax.fori_loop(0, BLOCKS, block, 0)

    def finish(i, carry):
        rows = pl.ds(pl.multiple_of(i * 512, 512), 512)
        dk_ref[rows, :] = acc_k[rows, :].astype(BF16)
        dv_ref[rows, :] = acc_v[rows, :].astype(BF16)
        return carry

    lax.fori_loop(0, SEQ // 512, finish, 0)


def run_chosen(chosen, k_all, v_all, q, g, gates, sums, dqp, dpk, dpv):
    vmem = pl.BlockSpec(memory_space=pltpu.VMEM)
    smem = pl.BlockSpec(memory_space=pltpu.SMEM)
    return pl.pallas_call(
        chosen_kernel,
        name="chosen",
        out_shape=(
            jax.ShapeDtypeStruct((TOKENS, GROUP * HEAD_DIM), BF16),
            jax.ShapeDtypeStruct((GROUP * HEAD_DIM, TOKENS), BF16),
            jax.ShapeDtypeStruct((SEQ, HEAD_DIM), BF16),
            jax.ShapeDtypeStruct((SEQ, HEAD_DIM), BF16),
        ),
        in_specs=[smem] + [vmem] * 9,
        out_specs=(vmem,) * 4,
        scratch_shapes=[
            pltpu.VMEM((SEQ, HEAD_DIM), F32),
            pltpu.VMEM((SEQ, HEAD_DIM), F32),
            pltpu.VMEM((CHOSEN * KEY_BLOCK, HEAD_DIM), BF16),
            pltpu.VMEM((CHOSEN * KEY_BLOCK, HEAD_DIM), BF16),
        ],
    )(chosen, k_all, v_all, q, g, gates, sums, dqp, dpk, dpv)


class Reduce:
    def __init__(self, send, axis, src, bufs, coords, along):
        (self.relay, self.direct, self.comb, self.out, self.total,
         self.relay2, self.direct2, self.comb2, self.out2) = bufs
        self.send, self.axis, self.src = send, axis, src
        self.c1, self.c2 = (coords[0], coords[1]) if axis == 0 else (coords[1], coords[0])
        self.to1 = lambda o: along(axis, o)
        self.to2 = lambda o: along(1 - axis, o)
        self.half = src.shape[2] // 2
        self.lo, self.hi = pl.ds(0, self.half), pl.ds(self.half, self.half)

    def bundle(self, o, rows):
        c = shifted(self.c1, o)
        return self.src.at[c, :, rows] if self.axis == 0 else self.src.at[:, c, rows]

    def piece(self, o, i, rows):
        c = shifted(self.c1, o)
        if self.axis == 0:
            return self.src[c, i, rows, :]
        return self.src[i, c, rows, :]

    def part(self, o, rows):
        return self.total.at[shifted(self.c2, o), rows]

    def begin(self):
        s = self.send
        self.r = [
            s(self.bundle(2, self.lo), self.relay.at[0], self.to1(1)),
            s(self.bundle(2, self.hi), self.relay.at[1], self.to1(-1)),
        ]
        self.d = [
            s(self.bundle(1, self.hi), self.direct.at[0], self.to1(1)),
            s(self.bundle(-1, self.lo), self.direct.at[1], self.to1(-1)),
        ]

    def combine(self):
        self.c = []
        for n, (o, rows) in enumerate(((1, self.lo), (-1, self.hi))):
            self.r[n].wait_recv()

            def add(i, carry, n=n, o=o, rows=rows):
                self.out[n, i] = (
                    self.piece(o, i, rows).astype(F32) + self.relay[n, i].astype(F32)
                ).astype(BF16)
                return carry

            lax.fori_loop(0, SIDE, add, 0)
            self.c.append(self.send(self.out.at[n], self.comb.at[n], self.to1(o)))

    def turn(self):
        for copy in self.d + self.c:
            copy.wait_recv()

        def add(i, carry):
            self.total[i, self.lo, :] = (
                self.piece(0, i, self.lo).astype(F32)
                + self.comb[0, i].astype(F32)
                + self.direct[1, i].astype(F32)
            ).astype(BF16)
            self.total[i, self.hi, :] = (
                self.piece(0, i, self.hi).astype(F32)
                + self.comb[1, i].astype(F32)
                + self.direct[0, i].astype(F32)
            ).astype(BF16)
            return carry

        lax.fori_loop(0, SIDE, add, 0)
        s = self.send
        self.r = [
            s(self.part(2, self.lo), self.relay2.at[0], self.to2(1)),
            s(self.part(2, self.hi), self.relay2.at[1], self.to2(-1)),
        ]
        self.d = [
            s(self.part(1, self.hi), self.direct2.at[0], self.to2(1)),
            s(self.part(-1, self.lo), self.direct2.at[1], self.to2(-1)),
        ]

    def combine2(self):
        self.c = []
        for n, (o, rows) in enumerate(((1, self.lo), (-1, self.hi))):
            self.r[n].wait_recv()
            self.out2[n] = (
                self.total[shifted(self.c2, o), rows, :].astype(F32) + self.relay2[n].astype(F32)
            ).astype(BF16)
            self.c.append(self.send(self.out2.at[n], self.comb2.at[n], self.to2(o)))

    def end(self):
        for copy in self.d + self.c:
            copy.wait_recv()
        own = self.c2
        low = (
            self.total[own, self.lo, :].astype(F32)
            + self.comb2[0].astype(F32)
            + self.direct2[1].astype(F32)
        )
        high = (
            self.total[own, self.hi, :].astype(F32)
            + self.comb2[1].astype(F32)
            + self.direct2[0].astype(F32)
        )
        return low, high


def reduce_buffers(rows, lanes):
    half = rows // 2
    wide = pltpu.VMEM((2, SIDE, half, lanes), BF16)
    slim = pltpu.VMEM((2, half, lanes), BF16)
    return [wide] * 4 + [pltpu.VMEM((SIDE, rows, lanes), BF16)] + [slim] * 4


REDUCE_BUFS = 9
GW_ROWS = GROUP * HEAD_DIM // 2
GW_COLS = MODEL // OWNERS


def scatter_kernel(dk_ref, dv_ref, h_ref, gqt_ref, gk_out, gv_out, gw_out, gw0, gw1, *rest):
    bufs = [rest[i * REDUCE_BUFS : (i + 1) * REDUCE_BUFS] for i in range(4)]
    send_sems, recv_sems = rest[4 * REDUCE_BUFS :]
    kv, tp, cz, cy, cx, core = place()

    def along(axis, o):
        if axis == 0:
            return (shifted(cz, o) * SIDE + cy, tp)
        return (cz * SIDE + shifted(cy, o), tp)

    meet([along(axis, o) for axis in (0, 1) for o in (1, -1)])
    send = Sender(send_sems, recv_sems)
    rk, rv, w0, w1 = [
        Reduce(send, axis, src, buf, (cz, cy), along)
        for axis, src, buf in zip((0, 1, 0, 1), (dk_ref, dv_ref, gw0, gw1), bufs)
    ]
    rk.begin()
    rv.begin()

    def product(j, carry):
        cols = pl.ds(pl.multiple_of(j * GW_COLS, GW_COLS), GW_COLS)
        part = dot(gqt_ref[...], h_ref[:, cols], NN).astype(BF16)
        gw0[j // SIDE, j % SIDE] = part[:GW_ROWS]
        gw1[j // SIDE, j % SIDE] = part[GW_ROWS:]
        return carry

    lax.fori_loop(0, OWNERS, product, 0)
    rk.combine()
    rv.combine()
    w0.begin()
    w1.begin()
    rk.turn()
    rv.turn()
    w0.combine()
    w1.combine()
    rk.combine2()
    rv.combine2()
    w0.turn()
    w1.turn()
    half = TOKENS // 2
    for r, out in ((rk, gk_out), (rv, gv_out)):
        low, high = r.end()
        out[:half, :] = low.astype(BF16)
        out[half:, :] = high.astype(BF16)
    w0.combine2()
    w1.combine2()
    half = GW_ROWS // 2
    for n, r in enumerate((w0, w1)):
        low, high = r.end()
        gw_out[:, n * GW_ROWS : n * GW_ROWS + half] = low.T
        gw_out[:, n * GW_ROWS + half : (n + 1) * GW_ROWS] = high.T
    send.finish()


SCATTER_COPIES = 4 * 12


def run_scatter(dk, dv, h_all, gqt):
    vmem = pl.BlockSpec(memory_space=pltpu.VMEM)
    return pl.pallas_call(
        scatter_kernel,
        name="scatter",
        out_shape=(
            jax.ShapeDtypeStruct((TOKENS, HEAD_DIM), BF16),
            jax.ShapeDtypeStruct((TOKENS, HEAD_DIM), BF16),
            jax.ShapeDtypeStruct((GW_COLS, GROUP * HEAD_DIM), F32),
        ),
        in_specs=[vmem] * 4,
        out_specs=(vmem,) * 3,
        scratch_shapes=[
            pltpu.VMEM((SIDE, SIDE, GW_ROWS, GW_COLS), BF16),
            pltpu.VMEM((SIDE, SIDE, GW_ROWS, GW_COLS), BF16),
            *reduce_buffers(TOKENS, HEAD_DIM),
            *reduce_buffers(TOKENS, HEAD_DIM),
            *reduce_buffers(GW_ROWS, GW_COLS),
            *reduce_buffers(GW_ROWS, GW_COLS),
            pltpu.SemaphoreType.DMA((SCATTER_COPIES,)),
            pltpu.SemaphoreType.DMA((SCATTER_COPIES,)),
        ],
        compiler_params=pltpu.CompilerParams(collective_id=1, has_side_effects=True),
    )(dk, dv, h_all, gqt)


def body(hidden_rows, queries, key_rows, value_rows, branch_gates, log_sums, chosen, out_grad):
    k_all, v_all, h_all, dqp, dpk, dpv = run_gather(
        key_rows, value_rows, hidden_rows, queries, out_grad, branch_gates, log_sums
    )
    gq, gqt, dk, dv = run_chosen(
        chosen.reshape(BLOCKS, CHOSEN),
        k_all.reshape(SEQ, HEAD_DIM),
        v_all.reshape(SEQ, HEAD_DIM),
        queries, out_grad, branch_gates, log_sums, dqp, dpk, dpv,
    )
    plane = (SIDE, SIDE, TOKENS, HEAD_DIM)
    gk, gv, gw = run_scatter(
        dk.reshape(plane), dv.reshape(plane), h_all.reshape(TOKENS, MODEL), gqt
    )
    return gq, gk, gv, gw


def solution(mesh):
    placed = (
        P(("kv", "tp"), None),
        P("kv", "tp"),
        P("kv", "tp"),
        P("kv", "tp"),
        P(None, "tp", "kv"),
        P(None, "tp", "kv"),
        P("tp", "kv", None),
        P("kv", "tp"),
    )
    return jax.shard_map(
        body,
        mesh=mesh,
        in_specs=placed,
        out_specs=(P("kv", "tp"), P("kv", "tp"), P("kv", "tp"), P("kv", "tp")),
        check_vma=False,
    )
```

time: 298 us -> 165 us (0.55)
  Pallas kernels: 0 us -> 159 us
  local copies, waits for them, and re-layouts: 81.8 us -> 5.21 us
  matrix products: 55 us -> 0 us
  waiting for transfers between devices: 49.5 us -> 0 us
  other arithmetic: 39 us -> 0 us
  starting transfers between devices: 29.8 us -> 0 us
  blocking collectives: 24.1 us -> 0 us
  between operations: 16 us -> 0.65 us
    pallas_call x0 -> x3, Pallas kernels: none -> 159 us  [the longest x1 75.7 us: run_scatter(): pl.pallas_call(scatter_kernel, name='scatter', out_shape=(jax.ShapeDtypeS...]
    dot_general x15 -> x0, matrix products: 55 us -> none  [the longest x2 11.7 us: attend_back(): jnp.einsum('bgrm,bgrd->bmd', weights_low, cotangent, preferred_element_ty...]
    all_to_all x5 -> x0, waiting for transfers between devices: 43.4 us -> none  [the longest x1 19.9 us: body(): lax.all_to_all(back_values.astype(jnp.bfloat16), 'kv', split_axis=1, conc...]
    scatter x3 -> x0, local copies, waits for them, and re-layouts: 34.3 us -> none  [the longest x1 17.6 us: body(): back_values = jnp.zeros((kv_local, slot_count, KEY_BLOCK, HEAD_DIM), jnp....]
    all_to_all x5 -> x0, starting transfers between devices: 29.5 us -> none  [the longest x1 8.16 us: body(): lax.all_to_all(wanted, 'kv', split_axis=1, concat_axis=1, tiled=True)]
    all_gather x1 -> x0, blocking collectives: 24.1 us -> none  [sent_together(): lax.all_gather(both, axis, axis=dim, tiled=True)]
    scatter-add x2 -> x0, other arithmetic: 17.8 us -> none  [the longest x1 11.9 us: body(): pick_dvalues = jnp.zeros((kv_local, blocks_here, KEY_BLOCK, HEAD_DIM), jn...]
    another operation x6 -> x0, local copies, waits for them, and re-layouts: 15.1 us -> none
  transfers between devices with their start and end apart: 8 -> 0, of which waited for: 4 -> 0; matrix products, arithmetic and copies ran while one was open for 57% -> 0% of each run, Pallas kernels for 0% -> 0%
where the time goes in v1:
time: 165 us
  Pallas kernels  159 us (96%)
  local copies, waits for them, and re-layouts  5.21 us (3%)
    pallas_call x1, Pallas kernels, run_scatter(): pl.pallas_call(scatter_kernel, name='scatter', out_shape=(jax.ShapeDtypeS...  75.7 us
    pallas_call x1, Pallas kernels, run_gather(): pl.pallas_call(gather_kernel, name='gather', out_shape=(jax.ShapeDtypeStr...  61.6 us
    pallas_call x1, Pallas kernels, run_chosen(): pl.pallas_call(chosen_kernel, name='chosen', out_shape=(jax.ShapeDtypeStr...  21.6 us
    unnamed x3, local copies, waits for them, and re-layouts  5.21 us

profile of v1, /device:TPU:0, one launch (start us, length us, event | category | flops | bytes accessed | tf_op | source)
XLA Modules:
  0.0 164.8 jit_solution(783452553942121820)
XLA Ops:
  0.6 61.6 %gather.1 = (bf16[16,1024,128]{2,1,0:T(8,128)(2,1)}, bf16[16,1024,128]{2,1,0:T(8,128)(2,1)}, bf16[8,128,4096]{2,1,0:T(8,128)(2,1)}, f32[8,128,512]{2,1,0:T(8,128...) custom-call(bf16[1024,128]{1,0:T(8,128)(2,1)} %k_ref.1, bf16[1024,128]{1,0:T(8,128)(2,1)} %v_ref.1, bf16[128,4096]{1,0:T(8,128)(2,1)} %h_ref.1, ...), custom_call_target="tpu_custom_call" | custom-call | tf_op jit(solution)/shard_map/gather/pallas_call | solution.py:255
  62.2 21.6 %chosen.1 = (bf16[1024,512]{1,0:T(8,128)(2,1)}, bf16[512,1024]{1,0:T(8,128)(2,1)}, bf16[16384,128]{1,0:T(8,128)(2,1)}, bf16[16384,128]{1,0:T(8,128)(2,1)}) custom-call(s32[8,16]{1,0:T(8,128)} %bitcast.11, bf16[16384,128]{1,0:T(8,128)(2,1)} %bitcast.9, bf16[16384,128]{1,0:T(8,128)(2,1)} %bitcast.10, bf16[1024,512]{1,0:T(8,128)(2,1)} %q_ref.3, ...), custom_call_target="tpu_custom_call" | custom-call | tf_op jit(solution)/shard_map/chosen/pallas_call | solution.py:350
  83.8 75.7 %scatter.1 = (bf16[1024,128]{1,0:T(8,128)(2,1)}, bf16[1024,128]{1,0:T(8,128)(2,1)}, f32[256,512]{1,0:T(8,128)}) custom-call(bf16[4,4,1024,128]{3,2,1,0:T(8,128)(2,1)} %bitcast.7, bf16[4,4,1024,128]{3,2,1,0:T(8,128)(2,1)} %bitcast.8, bf16[1024,4096]{1,0:T(8,128)(2,1)} %bitcast.6, bf16[512,1024]{1,0:T(8,128)(2,1)} %get-tuple-element.26.gqt_ref), custom_call_target="tpu_custom_call" | custom-call | tf_op jit(solution)/shard_map/scatter/pallas_call | solution.py:544
  159.6 1.7 %copy.15 = bf16[1024,128]{1,0:T(8,128)(2,1)} copy(bf16[1024,128]{1,0:T(8,128)(2,1)} %get-tuple-element.35) | data formatting | bytes 524288
  161.2 1.7 %copy.16 = bf16[1024,128]{1,0:T(8,128)(2,1)} copy(bf16[1024,128]{1,0:T(8,128)(2,1)} %get-tuple-element.36) | data formatting | bytes 524288
  162.9 1.9 %copy.17 = f32[256,512]{1,0:T(8,128)} copy(f32[256,512]{1,0:T(8,128)} %get-tuple-element.37) | data formatting | bytes 1048576

commit v2 on v1

--- a/solution.py
+++ b/solution.py
@@ -22,6 +22,7 @@
 MODEL = 4096
 SCALE = HEAD_DIM ** (-0.5)
 LOG2E = 1.4426950408889634
+MIB = 1 << 20
 MESH = pl.DeviceIdType.MESH
 F32 = jnp.float32
 BF16 = jnp.bfloat16
@@ -276,7 +277,9 @@
             pltpu.SemaphoreType.DMA((GATHER_COPIES,)),
             pltpu.SemaphoreType.DMA((3,)),
         ],
-        compiler_params=pltpu.CompilerParams(collective_id=0, has_side_effects=True),
+        compiler_params=pltpu.CompilerParams(
+            collective_id=0, has_side_effects=True, vmem_limit_bytes=12 * MIB
+        ),
     )(k, v, h, q, g, gates, sums)
 
 
@@ -364,6 +367,7 @@
             pltpu.VMEM((CHOSEN * KEY_BLOCK, HEAD_DIM), BF16),
             pltpu.VMEM((CHOSEN * KEY_BLOCK, HEAD_DIM), BF16),
         ],
+        compiler_params=pltpu.CompilerParams(vmem_limit_bytes=24 * MIB),
     )(chosen, k_all, v_all, q, g, gates, sums, dqp, dpk, dpv)
 
 
@@ -561,8 +565,28 @@
             pltpu.SemaphoreType.DMA((SCATTER_COPIES,)),
             pltpu.SemaphoreType.DMA((SCATTER_COPIES,)),
         ],
-        compiler_params=pltpu.CompilerParams(collective_id=1, has_side_effects=True),
+        compiler_params=pltpu.CompilerParams(
+            collective_id=1, has_side_effects=True, vmem_limit_bytes=24 * MIB
+        ),
     )(dk, dv, h_all, gqt)
+
+
+def finish_kernel(gk_ref, gv_ref, gw_ref, gk_out, gv_out, gw_out):
+    gk_out[...] = gk_ref[...]
+    gv_out[...] = gv_ref[...]
+    gw_out[...] = gw_ref[...]
+
+
+def run_finish(gk, gv, gw):
+    vmem = pl.BlockSpec(memory_space=pltpu.VMEM)
+    return pl.pallas_call(
+        finish_kernel,
+        name="finish",
+        out_shape=tuple(jax.ShapeDtypeStruct(a.shape, a.dtype) for a in (gk, gv, gw)),
+        in_specs=[vmem] * 3,
+        out_specs=(vmem,) * 3,
+        compiler_params=pltpu.CompilerParams(vmem_limit_bytes=8 * MIB),
+    )(gk, gv, gw)
 
 
 def body(hidden_rows, queries, key_rows, value_rows, branch_gates, log_sums, chosen, out_grad):
@@ -579,6 +603,7 @@
     gk, gv, gw = run_scatter(
         dk.reshape(plane), dv.reshape(plane), h_all.reshape(TOKENS, MODEL), gqt
     )
+    gk, gv, gw = run_finish(gk, gv, gw)
     return gq, gk, gv, gw
 
 

time: 165 us -> 152 us (0.921)
  Pallas kernels: 159 us -> 142 us
  local copies, waits for them, and re-layouts: 5.21 us -> 9.28 us
    pallas_call x1, Pallas kernels: 21.6 us -> 14.5 us  [run_chosen(): pl.pallas_call(chosen_kernel, name='chosen', out_shape=(jax.ShapeDtypeStr...]
    pallas_call x1, Pallas kernels: 75.7 us -> 68.7 us  [run_scatter(): pl.pallas_call(scatter_kernel, name='scatter', out_shape=(jax.ShapeDtypeS...]
    pallas_call x1, Pallas kernels: 61.6 us -> 57.4 us  [run_gather(): pl.pallas_call(gather_kernel, name='gather', out_shape=(jax.ShapeDtypeStr...]
    unnamed x3 -> x24, local copies, waits for them, and re-layouts: 5.21 us -> 9.28 us
where the time goes in v2:
time: 152 us
  Pallas kernels  142 us (93%)
  local copies, waits for them, and re-layouts  9.28 us (6%)
    pallas_call x1, Pallas kernels, run_scatter(): pl.pallas_call(scatter_kernel, name='scatter', out_shape=(jax.ShapeDtypeS...  68.7 us
    pallas_call x1, Pallas kernels, run_gather(): pl.pallas_call(gather_kernel, name='gather', out_shape=(jax.ShapeDtypeStr...  57.4 us
    pallas_call x1, Pallas kernels, run_chosen(): pl.pallas_call(chosen_kernel, name='chosen', out_shape=(jax.ShapeDtypeStr...  14.5 us
    unnamed x24, local copies, waits for them, and re-layouts  9.28 us

profile of v2, /device:TPU:0, one launch (start us, length us, event | category | flops | bytes accessed | tf_op | source)
XLA Modules:
  0.0 151.6 jit_solution(10314942073669529143)
XLA Ops:
  0.6 0.0 copy-start
  0.6 1.2 copy-done
  1.9 0.0 copy-start.2
  1.9 1.2 copy-done.2
  3.1 0.0 copy-start.4
  3.1 1.2 copy-done.4
  4.3 0.0 copy-start.5
  4.3 0.9 copy-done.5
  5.3 0.0 copy-start.6
  5.3 0.9 copy-done.6
  6.2 0.0 copy-start.7
  6.2 0.8 copy-done.7
  7.0 0.0 copy-start.9
  7.0 0.8 copy-done.9
  7.7 0.0 copy-start.1
  7.7 0.0 copy-start.3
  7.7 57.4 %gather.1 = (bf16[16,1024,128]{2,1,0:T(8,128)(2,1)S(1)}, bf16[16,1024,128]{2,1,0:T(8,128)(2,1)S(1)}, bf16[8,128,4096]{2,1,0:T(8,128)(2,1)S(1)}, f32[8,128,512]{2...) custom-call(bf16[1024,128]{1,0:T(8,128)(2,1)S(1)} %copy-done.5, bf16[1024,128]{1,0:T(8,128)(2,1)S(1)} %copy-done.6, ...), custom_call_target="tpu_custom_call" | custom-call | tf_op jit(solution)/shard_map/gather/pallas_call | solution.py:256
  65.1 0.0 copy-done.1
  65.1 0.0 copy-done.3
  65.2 0.0 copy-start.8
  65.2 0.7 copy-done.8
  65.9 0.0 copy-start.10
  65.9 0.8 copy-done.10
  66.7 0.0 copy-start.11
  66.7 0.7 copy-done.11
  67.4 14.5 %chosen.1 = (bf16[1024,512]{1,0:T(8,128)(2,1)}, bf16[512,1024]{1,0:T(8,128)(2,1)S(1)}, bf16[16384,128]{1,0:T(8,128)(2,1)S(1)}, bf16[16384,128]{1,0:T(8,128)(2,1)S(1)}) custom-call(s32[8,16]{1,0:T(8,128)S(1)} %bitcast.11, bf16[16384,128]{1,0:T(8,128)(2,1)S(1)} %bitcast.9, bf16[16384,128]{1,0:T(8,128)(2,1)S(1)} %bitcast.10, bf16[1024,512]{1,0:T(8,128)(2,1)S(1)} %copy-done.1, ...), custom_call_target="tpu_custom_call" | custom-call | tf_op jit(solution)/shard_map/chosen/pallas_call | solution.py:353
  81.8 68.7 %scatter.1 = (bf16[1024,128]{1,0:T(8,128)(2,1)S(1)}, bf16[1024,128]{1,0:T(8,128)(2,1)S(1)}, f32[256,512]{1,0:T(8,128)S(1)}) custom-call(bf16[4,4,1024,128]{3,2,1,0:T(8,128)(2,1)S(1)} %bitcast.7, bf16[4,4,1024,128]{3,2,1,0:T(8,128)(2,1)S(1)} %bitcast.8, bf16[1024,4096]{1,0:T(8,128)(2,1)S(1)} %bitcast.6, bf16[512,1024]{1,0:T(8,128)(2,1)S(1)} %get-tuple-element.29.gqt_ref), custom_call_target="tpu_custom_call" | custom-call | tf_op jit(solution)/shard_map/scatter/pallas_call | solution.py:548
  150.5 1.0 finish.1
Async XLA Ops:
  0.6 1.2 copy-start
  1.9 1.2 copy-start.2
  3.1 1.2 copy-start.4
  4.3 0.9 copy-start.5
  5.3 0.9 copy-start.6
  6.2 0.8 copy-start.7
  7.0 0.8 copy-start.9
  7.7 57.4 %copy-start.1 = (bf16[1024,512]{1,0:T(8,128)(2,1)S(1)}, bf16[1024,512]{1,0:T(8,128)(2,1)}, u32[]{:S(2)}) copy-start(bf16[1024,512]{1,0:T(8,128)(2,1)} %q_ref.3) | copy-start | bytes 3145732
  7.7 57.4 %copy-start.3 = (bf16[1024,512]{1,0:T(8,128)(2,1)S(1)}, bf16[1024,512]{1,0:T(8,128)(2,1)}, u32[]{:S(2)}) copy-start(bf16[1024,512]{1,0:T(8,128)(2,1)} %g_ref.3) | copy-start | bytes 3145732
  65.2 0.8 copy-start.8
  65.9 0.8 copy-start.10
  66.7 0.7 copy-start.11

commit v3 on v2

v3 whole, which is shorter than its diff:
```python
import jax
import jax.numpy as jnp
from jax import lax
from jax.experimental import pallas as pl
from jax.experimental.pallas import tpu as pltpu
from jax.sharding import PartitionSpec as P

HEADS = 32
KV_HEADS = 8
HEAD_DIM = 128
QUERY_BLOCK = 128
KEY_BLOCK = 32
POOL_BLOCK = 32
CHOSEN = 16
GROUP = HEADS // KV_HEADS
SIDE = 4
OWNERS = SIDE * SIDE
TOKENS = 1024
BLOCKS = TOKENS // QUERY_BLOCK
POOLED = TOKENS // POOL_BLOCK
SEQ = TOKENS * OWNERS
MODEL = 4096
SCALE = HEAD_DIM ** (-0.5)
LOG2E = 1.4426950408889634
MIB = 1 << 20
MESH = pl.DeviceIdType.MESH
F32 = jnp.float32
BF16 = jnp.bfloat16

NT = (((1,), (1,)), ((), ()))
NN = (((1,), (0,)), ((), ()))


def dot(a, b, dims):
    return lax.dot_general(a, b, dims, preferred_element_type=F32)


class Sender:
    def __init__(self, send_sems, recv_sems):
        self.send_sems, self.recv_sems, self.at, self.sent = send_sems, recv_sems, 0, []

    def __call__(self, src, dst, dev):
        copy = pltpu.make_async_remote_copy(
            src_ref=src,
            dst_ref=dst,
            send_sem=self.send_sems.at[self.at],
            recv_sem=self.recv_sems.at[self.at],
            device_id=dev,
            device_id_type=MESH,
        )
        self.at += 1
        copy.start()
        self.sent.append(copy)
        return copy

    def finish(self):
        for copy in self.sent:
            copy.wait_send()


def place():
    kv, tp = lax.axis_index("kv"), lax.axis_index("tp")
    return kv, tp, kv // SIDE, kv % SIDE, tp // 2, tp % 2


def shifted(c, o):
    return (c + (o + SIDE)) % SIDE


def greet(devices):
    for dev in devices:
        pl.semaphore_signal(
            pltpu.get_barrier_semaphore(), inc=1, device_id=dev, device_id_type=MESH
        )


def meet(count):
    pl.semaphore_wait(pltpu.get_barrier_semaphore(), count)


def tile_operands(q_ref, g_ref, gate_ref, ls_ref, t):
    rows = pl.ds(pl.multiple_of(t * QUERY_BLOCK, QUERY_BLOCK), QUERY_BLOCK)
    gates = jnp.concatenate([gate_ref[0, :, rows], gate_ref[1, :, rows]], axis=0).T
    qs, cs, ls = [], ([], []), ([], [])
    for h in range(GROUP):
        cols = slice(h * HEAD_DIM, (h + 1) * HEAD_DIM)
        qs.append(q_ref[rows, cols])
        grad = g_ref[rows, cols].astype(F32)
        for branch in (0, 1):
            at = branch * GROUP + h
            cs[branch].append((gates[:, at : at + 1] * grad).astype(BF16))
            ls[branch].append(ls_ref[branch, h : h + 1, rows])
    return (
        jnp.concatenate(qs, axis=0),
        [jnp.concatenate(c, axis=0) for c in cs],
        [jnp.concatenate(x, axis=1) * LOG2E for x in ls],
    )


def attend_back(qs, cs, log_sum, keys, values, visible):
    scores = dot(keys, qs, NT) * (SCALE * LOG2E)
    p = jnp.where(visible, jnp.exp2(scores - log_sum), 0.0)
    pr = p.astype(BF16)
    dp = dot(values, cs, NT)
    delta = jnp.sum(pr.astype(F32) * dp, axis=0, keepdims=True)
    ds = (p * (dp - delta)).astype(BF16)
    return dot(keys.T, ds, NN), dot(ds, qs, NN), dot(pr, cs, NN)


def gather_kernel(
    k_ref, v_ref, h_ref, q_hbm, g_hbm, gate_hbm, ls_hbm,
    k_all, v_all, h_all, dq_ref, dpk_ref, dpv_ref, qs_all, cs_all, ls_rows,
    q_ref, g_ref, gate_ref, ls_ref, pool_all, pk_ref, pv_ref, pool_here,
    pool_send, pool_recv, send_sems, recv_sems, local_sems,
):
    kv, tp, cz, cy, cx, core = place()
    half = TOKENS // 2

    def device(oz, oy):
        return (shifted(cz, oz) * SIDE + shifted(cy, oy), tp)

    def along(axis, o):
        return device(o, 0) if axis == 0 else device(0, o)

    def owner(axis, o1, o2):
        a, b = (o1, o2) if axis == 0 else (o2, o1)
        return shifted(cz, a) * SIDE + shifted(cy, b)

    def xdev(o, c):
        return (kv, shifted(cx, o) * 2 + c)

    others = [(oz, oy) for oz in range(SIDE) for oy in range(SIDE) if (oz, oy) != (0, 0)]
    peers = [device(oz, oy) for oz, oy in others] + [
        xdev(1, core), xdev(-1, core), xdev(0, 1 - core)
    ]
    greet(peers)
    local = [
        pltpu.make_async_copy(src, dst, local_sems.at[i])
        for i, (src, dst) in enumerate(
            (
                (k_ref, k_all.at[kv]),
                (v_ref, v_all.at[kv]),
                (h_ref, h_all.at[tp]),
                (gate_hbm, gate_ref),
                (ls_hbm, ls_ref),
                (q_hbm, q_ref),
                (g_hbm, g_ref),
            )
        )
    ]
    for copy in local:
        copy.start()

    blk = lax.broadcasted_iota(jnp.int32, (POOLED, TOKENS), 0)
    row = lax.broadcasted_iota(jnp.int32, (POOLED, TOKENS), 1)
    mean = jnp.where(row // POOL_BLOCK == blk, 1.0 / POOL_BLOCK, 0.0).astype(BF16)
    local[0].wait()
    pool_here[0] = dot(mean, k_all[kv], NN).astype(BF16)
    local[1].wait()
    pool_here[1] = dot(mean, v_all[kv], NN).astype(BF16)
    meet(len(peers))

    pool_sender = Sender(pool_send, pool_recv)
    for oz, oy in others:
        pool_sender(pool_here, pool_all.at[kv], device(oz, oy))
    pool_all[kv] = pool_here[...]

    send = Sender(send_sems, recv_sems)
    first, wide = {}, {}
    arrays = ((0, k_all), (1, v_all))
    for axis, full in arrays:
        here = full.at[kv]
        first[axis] = [send(here, here, along(axis, s)) for s in (1, -1)]
    local[2].wait()
    here = h_all.at[tp]
    x_first = [send(here, here, xdev(s, core)) for s in (1, -1)]
    x_over = [send(here, here, xdev(0, 1 - core))]
    for axis, full in arrays:
        here = full.at[kv]
        wide[axis] = [(0, [send(here, here, along(1 - axis, s)) for s in (1, -1)])]

    for copy in local[3:]:
        copy.wait()
    for copy in pool_sender.sent:
        copy.wait_recv()
    pk_ref[...] = pool_all[:, 0].reshape(OWNERS * POOLED, HEAD_DIM)
    pv_ref[...] = pool_all[:, 1].reshape(OWNERS * POOLED, HEAD_DIM)
    dpk_ref[...] = jnp.zeros_like(dpk_ref)
    dpv_ref[...] = jnp.zeros_like(dpv_ref)

    n_pool = OWNERS * POOLED
    wide_q = GROUP * QUERY_BLOCK
    pool_end = lax.broadcasted_iota(jnp.int32, (n_pool, wide_q), 0) * POOL_BLOCK + POOL_BLOCK - 1
    lane = lax.broadcasted_iota(jnp.int32, (n_pool, wide_q), 1) % QUERY_BLOCK
    ahead = pool_end - lane

    def tile(t, carry):
        qs, cs, ls = tile_operands(q_ref, g_ref, gate_ref, ls_ref, t)
        qs_all[t] = qs
        cs_all[t] = cs[1]
        ls_rows[t] = ls[1]
        visible = ahead <= kv * TOKENS + t * QUERY_BLOCK
        dq, dk, dv = attend_back(qs, cs[0], ls[0], pk_ref[...], pv_ref[...], visible)
        dq_ref[t] = dq
        dpk_ref[...] += dk
        dpv_ref[...] += dv
        return carry

    lax.fori_loop(0, 4, tile, 0)

    second = {}
    for axis, full in arrays:
        plus, minus = first[axis]
        plus.wait_recv()
        part = full.at[owner(axis, -1, 0), pl.ds(0, half)]
        fwd = send(part, part, along(axis, 1))
        whole = full.at[owner(axis, -1, 0)]
        wide[axis].append((-1, [send(whole, whole, along(1 - axis, s)) for s in (1, -1)]))
        minus.wait_recv()
        part = full.at[owner(axis, 1, 0), pl.ds(half, half)]
        bwd = send(part, part, along(axis, -1))
        whole = full.at[owner(axis, 1, 0)]
        wide[axis].append((1, [send(whole, whole, along(1 - axis, s)) for s in (1, -1)]))
        second[axis] = (fwd, bwd)

    lax.fori_loop(4, BLOCKS, tile, 0)
    dpk_ref[...] = dpk_ref[...] * (SCALE / POOL_BLOCK)
    dpv_ref[...] = dpv_ref[...] * (1.0 / POOL_BLOCK)

    last = []

    def across(axis, full, o, pair):
        plus, minus = pair
        plus.wait_recv()
        part = full.at[owner(axis, o, -1), pl.ds(0, half)]
        last.append(send(part, part, along(1 - axis, 1)))
        minus.wait_recv()
        part = full.at[owner(axis, o, 1), pl.ds(half, half)]
        last.append(send(part, part, along(1 - axis, -1)))

    for axis, full in arrays:
        across(axis, full, *wide[axis][0])
    for axis, full in arrays:
        for copy in second[axis]:
            copy.wait_recv()
        whole = full.at[owner(axis, 2, 0)]
        wide[axis].append((2, [send(whole, whole, along(1 - axis, s)) for s in (1, -1)]))
    rows = TOKENS // 16
    plus, minus = x_first
    plus.wait_recv()
    whole = h_all.at[shifted(cx, -1) * 2 + core]
    part = whole.at[pl.ds(0, rows)]
    x_second = [send(part, part, xdev(1, core))]
    x_over.append(send(whole, whole, xdev(0, 1 - core)))
    minus.wait_recv()
    whole = h_all.at[shifted(cx, 1) * 2 + core]
    part = whole.at[pl.ds(rows, rows)]
    x_second.append(send(part, part, xdev(-1, core)))
    x_over.append(send(whole, whole, xdev(0, 1 - core)))
    for i in (1, 2):
        for axis, full in arrays:
            across(axis, full, *wide[axis][i])
    for copy in x_second:
        copy.wait_recv()
    whole = h_all.at[shifted(cx, 2) * 2 + core]
    x_over.append(send(whole, whole, xdev(0, 1 - core)))
    for axis, full in arrays:
        across(axis, full, *wide[axis][3])
    for copy in last:
        copy.wait_recv()
    for copy in x_over:
        copy.wait_recv()
    pool_sender.finish()
    send.finish()


GATHER_COPIES = 2 * (2 + 2 + 8 + 8) + 2 + 2 + 4


def run_gather(k, v, h, q, g, gates, sums):
    hbm = pl.BlockSpec(memory_space=pltpu.HBM)
    vmem = pl.BlockSpec(memory_space=pltpu.VMEM)
    n_pool = OWNERS * POOLED
    wide_q = GROUP * QUERY_BLOCK
    return pl.pallas_call(
        gather_kernel,
        name="gather",
        out_shape=(
            jax.ShapeDtypeStruct((OWNERS, TOKENS, HEAD_DIM), BF16),
            jax.ShapeDtypeStruct((OWNERS, TOKENS, HEAD_DIM), BF16),
            jax.ShapeDtypeStruct((8, TOKENS // 8, MODEL), BF16),
            jax.ShapeDtypeStruct((BLOCKS, HEAD_DIM, wide_q), F32),
            jax.ShapeDtypeStruct((n_pool, HEAD_DIM), F32),
            jax.ShapeDtypeStruct((n_pool, HEAD_DIM), F32),
            jax.ShapeDtypeStruct((BLOCKS, wide_q, HEAD_DIM), BF16),
            jax.ShapeDtypeStruct((BLOCKS, wide_q, HEAD_DIM), BF16),
            jax.ShapeDtypeStruct((BLOCKS, 1, wide_q), F32),
        ),
        in_specs=[hbm] * 7,
        out_specs=(vmem,) * 9,
        scratch_shapes=[
            pltpu.VMEM(q.shape, BF16),
            pltpu.VMEM(g.shape, BF16),
            pltpu.VMEM(gates.shape, F32),
            pltpu.VMEM(sums.shape, F32),
            pltpu.VMEM((OWNERS, 2, POOLED, HEAD_DIM), BF16),
            pltpu.VMEM((n_pool, HEAD_DIM), BF16),
            pltpu.VMEM((n_pool, HEAD_DIM), BF16),
            pltpu.VMEM((2, POOLED, HEAD_DIM), BF16),
            pltpu.SemaphoreType.DMA((OWNERS - 1,)),
            pltpu.SemaphoreType.DMA((OWNERS - 1,)),
            pltpu.SemaphoreType.DMA((GATHER_COPIES,)),
            pltpu.SemaphoreType.DMA((GATHER_COPIES,)),
            pltpu.SemaphoreType.DMA((7,)),
        ],
        compiler_params=pltpu.CompilerParams(
            collective_id=0, has_side_effects=True, vmem_limit_bytes=12 * MIB
        ),
        cost_estimate=pl.CostEstimate(
            flops=40_000_000_000, bytes_accessed=8 * MIB, transcendentals=0
        ),
    )(*(pltpu.with_memory_space_constraint(a, pltpu.HBM) for a in (k, v, h, q, g, gates, sums)))


class Reduce:
    def __init__(self, send, axis, src, bufs, coords, along):
        self.relay, self.direct, self.comb, self.relay2, self.direct2, self.comb2 = bufs
        self.send, self.axis, self.src = send, axis, src
        self.c1, self.c2 = (coords[0], coords[1]) if axis == 0 else (coords[1], coords[0])
        self.to1 = lambda o: along(axis, o)
        self.to2 = lambda o: along(1 - axis, o)
        self.half = src.shape[2] // 2
        self.rows = (pl.ds(0, self.half), pl.ds(self.half, self.half))

    def bundle(self, o, n):
        c = shifted(self.c1, o)
        rows = self.rows[n]
        return self.src.at[c, :, rows] if self.axis == 0 else self.src.at[:, c, rows]

    def piece(self, o, i, n):
        c = shifted(self.c1, o)
        if self.axis == 0:
            return self.src[c, i, self.rows[n], :].astype(F32)
        return self.src[i, c, self.rows[n], :].astype(F32)

    def part(self, o, n):
        return self.comb.at[n, shifted(self.c2, o)]

    def begin(self):
        s = self.send
        self.r = [
            s(self.bundle(2, 0), self.relay.at[0], self.to1(1)),
            s(self.bundle(2, 1), self.relay.at[1], self.to1(-1)),
        ]
        self.d = [
            s(self.bundle(1, 1), self.direct.at[0], self.to1(1)),
            s(self.bundle(-1, 0), self.direct.at[1], self.to1(-1)),
        ]

    def combine(self):
        self.c = []
        for n, o in enumerate((1, -1)):
            self.r[n].wait_recv()

            def add(i, carry, n=n, o=o):
                self.relay[n, i] = (self.piece(o, i, n) + self.relay[n, i].astype(F32)).astype(BF16)
                return carry

            lax.fori_loop(0, SIDE, add, 0)
            self.c.append(self.send(self.relay.at[n], self.comb.at[n], self.to1(o)))

    def turn(self):
        for copy in self.d + self.c:
            copy.wait_recv()

        def add(i, carry):
            for n in (0, 1):
                self.comb[n, i] = (
                    self.piece(0, i, n)
                    + self.comb[n, i].astype(F32)
                    + self.direct[1 - n, i].astype(F32)
                ).astype(BF16)
            return carry

        lax.fori_loop(0, SIDE, add, 0)
        s = self.send
        self.r = [
            s(self.part(2, 0), self.relay2.at[0], self.to2(1)),
            s(self.part(2, 1), self.relay2.at[1], self.to2(-1)),
        ]
        self.d = [
            s(self.part(1, 1), self.direct2.at[0], self.to2(1)),
            s(self.part(-1, 0), self.direct2.at[1], self.to2(-1)),
        ]

    def combine2(self):
        self.c = []
        for n, o in enumerate((1, -1)):
            self.r[n].wait_recv()
            self.relay2[n] = (
                self.comb[n, shifted(self.c2, o)].astype(F32) + self.relay2[n].astype(F32)
            ).astype(BF16)
            self.c.append(self.send(self.relay2.at[n], self.comb2.at[n], self.to2(o)))

    def end(self):
        for copy in self.d + self.c:
            copy.wait_recv()
        return [
            self.comb[n, self.c2].astype(F32)
            + self.comb2[n].astype(F32)
            + self.direct2[1 - n].astype(F32)
            for n in (0, 1)
        ]


def reduce_buffers(rows, lanes):
    half = rows // 2
    wide = pltpu.VMEM((2, SIDE, half, lanes), BF16)
    slim = pltpu.VMEM((2, half, lanes), BF16)
    return [wide] * 3 + [slim] * 3


REDUCE_BUFS = 6
GW_COLS = MODEL // OWNERS
PAIR = GROUP // 2 * HEAD_DIM
PAIR_Q = GROUP // 2 * QUERY_BLOCK
SETS = CHOSEN * KEY_BLOCK


def scatter_kernel(
    chosen_ref, k_ref, v_ref, h_ref, dqp_ref, dpk_ref, dpv_ref, qs_all, cs_all, ls_rows,
    gq_ref, gk_out, gv_out, gw_out,
    kb, vb, dk_set, dv_set, gqt, dk_all, dv_all, gw0, gw1, gw2, gw3, order, *rest
):
    bufs = [rest[i * REDUCE_BUFS : (i + 1) * REDUCE_BUFS] for i in range(6)]
    send_sems, recv_sems = rest[6 * REDUCE_BUFS :]
    kv, tp, cz, cy, cx, core = place()

    def along(axis, o):
        if axis == 0:
            return (shifted(cz, o) * SIDE + cy, tp)
        return (cz * SIDE + shifted(cy, o), tp)

    peers = [along(axis, o) for axis in (0, 1) for o in (1, -1)]
    greet(peers)
    send = Sender(send_sems, recv_sems)
    gws = (gw0, gw1, gw2, gw3)
    rk, rv, w0, w1, w2, w3 = [
        Reduce(send, axis, src, buf, (cz, cy), along)
        for axis, src, buf in zip((0, 1, 0, 1, 0, 1), (dk_all, dv_all) + gws, bufs)
    ]

    ahead = (
        lax.broadcasted_iota(jnp.int32, (KEY_BLOCK, PAIR_Q), 0)
        - lax.broadcasted_iota(jnp.int32, (KEY_BLOCK, PAIR_Q), 1) % QUERY_BLOCK
    )

    def attend(pair):
        across = slice(pair * PAIR_Q, (pair + 1) * PAIR_Q)

        def block(b, carry):
            start_row = kv * TOKENS + b * QUERY_BLOCK
            seen = []
            for c in range(CHOSEN):
                at = chosen_ref[b, c]
                kb[c * KEY_BLOCK : (c + 1) * KEY_BLOCK, :] = k_ref[at]
                vb[c * KEY_BLOCK : (c + 1) * KEY_BLOCK, :] = v_ref[at]
                seen.append(ahead <= start_row - at * KEY_BLOCK)
            dq, dk, dv = attend_back(
                qs_all[b, across, :],
                cs_all[b, across, :],
                ls_rows[b, :, across],
                kb[...],
                vb[...],
                jnp.concatenate(seen, axis=0),
            )
            total = (dqp_ref[b, :, across] + dq) * SCALE
            rows = pl.ds(pl.multiple_of(b * QUERY_BLOCK, QUERY_BLOCK), QUERY_BLOCK)
            for h in range(GROUP // 2):
                part = total[:, h * QUERY_BLOCK : (h + 1) * QUERY_BLOCK]
                at = pair * PAIR + h * HEAD_DIM
                gqt[at : at + HEAD_DIM, rows] = part.astype(BF16)
                gq_ref[rows, at : at + HEAD_DIM] = part.T.astype(BF16)
            here = pl.ds(pl.multiple_of(b * SETS, SETS), SETS)
            if pair == 0:
                dk_set[here, :] = dk
                dv_set[here, :] = dv
            else:
                dk_set[here, :] += dk
                dv_set[here, :] += dv
            return carry

        return block

    def product(pair):
        def one(j, carry):
            cols = pl.ds(pl.multiple_of(j * GW_COLS, GW_COLS), GW_COLS)
            part = dot(gqt[pair * PAIR : (pair + 1) * PAIR, :], h_ref[:, cols], NN).astype(BF16)
            gws[2 * pair][j // SIDE, j % SIDE] = part[:HEAD_DIM]
            gws[2 * pair + 1][j // SIDE, j % SIDE] = part[HEAD_DIM:]
            return carry

        lax.fori_loop(0, OWNERS, one, 0)

    lax.fori_loop(0, BLOCKS, attend(0), 0)
    product(0)
    meet(len(peers))
    w0.begin()
    w1.begin()
    lax.fori_loop(0, BLOCKS // 2, attend(1), 0)
    w0.combine()
    w1.combine()
    lax.fori_loop(BLOCKS // 2, BLOCKS, attend(1), 0)

    lane = lax.broadcasted_iota(jnp.int32, (1, BLOCKS * CHOSEN), 1)
    listed = jnp.zeros((1, BLOCKS * CHOSEN), jnp.int32)
    for b in range(BLOCKS):
        for c in range(CHOSEN):
            listed = jnp.where(lane == b * CHOSEN + c, chosen_ref[b, c], listed)
    n_pool = OWNERS * POOLED
    hits = lax.broadcasted_iota(jnp.int32, (n_pool, BLOCKS * CHOSEN), 0) == listed
    hits = jnp.where(hits, 1.0, 0.0).astype(BF16)
    plane = (SIDE, SIDE, POOLED, HEAD_DIM)

    def spread(r, carry):
        every = pl.ds(r, BLOCKS * CHOSEN, stride=KEY_BLOCK)
        part = jnp.concatenate([dk_set[every, :], dv_set[every, :]], axis=1).astype(BF16)
        got = dot(hits, part, NN)
        rows = pl.ds(pl.multiple_of(r * POOLED, POOLED), POOLED)
        dk = got[:, :HEAD_DIM] * SCALE + dpk_ref[...]
        dv = got[:, HEAD_DIM:] + dpv_ref[...]
        dk_all[:, :, rows, :] = dk.astype(BF16).reshape(plane)
        dv_all[:, :, rows, :] = dv.astype(BF16).reshape(plane)
        return carry

    lax.fori_loop(0, KEY_BLOCK, spread, 0)
    rk.begin()
    rv.begin()
    w0.turn()
    w1.turn()
    product(1)
    rk.combine()
    rv.combine()
    w2.begin()
    w3.begin()
    w0.combine2()
    w1.combine2()
    rk.turn()
    rv.turn()
    w2.combine()
    w3.combine()
    rk.combine2()
    rv.combine2()
    w2.turn()
    w3.turn()

    def weight(n, w):
        for i, part in enumerate(w.end()):
            at = n * HEAD_DIM + i * HEAD_DIM // 2
            gw_out[:, at : at + HEAD_DIM // 2] = part.T

    weight(0, w0)
    weight(1, w1)
    for r, out in ((rk, gk_out), (rv, gv_out)):
        for n, part in enumerate(r.end()):
            for i in range(KEY_BLOCK // 2):
                at = n * (KEY_BLOCK // 2) + i
                order[pl.ds(at, POOLED, stride=KEY_BLOCK), :] = part[i * POOLED : (i + 1) * POOLED]
        out[...] = order[...].astype(BF16)
    w2.combine2()
    w3.combine2()
    weight(2, w2)
    weight(3, w3)
    send.finish()


SCATTER_COPIES = 6 * 12
SCATTER_MIB = 31


def run_scatter(chosen, k_all, v_all, h_all, dqp, dpk, dpv, qs, cs, ls):
    vmem = pl.BlockSpec(memory_space=pltpu.VMEM)
    smem = pl.BlockSpec(memory_space=pltpu.SMEM)
    dense = pltpu.VMEM((SIDE, SIDE, TOKENS, HEAD_DIM), BF16)
    grad = pltpu.VMEM((SIDE, SIDE, HEAD_DIM, GW_COLS), BF16)
    return pl.pallas_call(
        scatter_kernel,
        name="scatter",
        out_shape=(
            jax.ShapeDtypeStruct((TOKENS, GROUP * HEAD_DIM), BF16),
            jax.ShapeDtypeStruct((TOKENS, HEAD_DIM), BF16),
            jax.ShapeDtypeStruct((TOKENS, HEAD_DIM), BF16),
            jax.ShapeDtypeStruct((GW_COLS, GROUP * HEAD_DIM), F32),
        ),
        in_specs=[smem] + [vmem] * 9,
        out_specs=(vmem,) * 4,
        scratch_shapes=[
            pltpu.VMEM((SETS, HEAD_DIM), BF16),
            pltpu.VMEM((SETS, HEAD_DIM), BF16),
            pltpu.VMEM((BLOCKS * SETS, HEAD_DIM), F32),
            pltpu.VMEM((BLOCKS * SETS, HEAD_DIM), F32),
            pltpu.VMEM((GROUP * HEAD_DIM, TOKENS), BF16),
            dense,
            dense,
            grad,
            grad,
            grad,
            grad,
            pltpu.VMEM((TOKENS, HEAD_DIM), F32),
            *reduce_buffers(TOKENS, HEAD_DIM),
            *reduce_buffers(TOKENS, HEAD_DIM),
            *(reduce_buffers(HEAD_DIM, GW_COLS) * 4),
            pltpu.SemaphoreType.DMA((SCATTER_COPIES,)),
            pltpu.SemaphoreType.DMA((SCATTER_COPIES,)),
        ],
        compiler_params=pltpu.CompilerParams(
            collective_id=1, has_side_effects=True, vmem_limit_bytes=SCATTER_MIB * MIB
        ),
    )(chosen, k_all, v_all, h_all, dqp, dpk, dpv, qs, cs, ls)


def finish_kernel(*refs):
    for src, out in zip(refs[:4], refs[4:]):
        out[...] = src[...]


def run_finish(*outs):
    vmem = pl.BlockSpec(memory_space=pltpu.VMEM)
    return pl.pallas_call(
        finish_kernel,
        name="finish",
        out_shape=tuple(jax.ShapeDtypeStruct(a.shape, a.dtype) for a in outs),
        in_specs=[vmem] * 4,
        out_specs=(vmem,) * 4,
        compiler_params=pltpu.CompilerParams(vmem_limit_bytes=8 * MIB),
    )(*outs)


def body(hidden_rows, queries, key_rows, value_rows, branch_gates, log_sums, chosen, out_grad):
    k_all, v_all, h_all, *pooled = run_gather(
        key_rows, value_rows, hidden_rows, queries, out_grad, branch_gates, log_sums
    )
    outs = run_scatter(
        chosen.reshape(BLOCKS, CHOSEN),
        k_all.reshape(SEQ // KEY_BLOCK, KEY_BLOCK, HEAD_DIM),
        v_all.reshape(SEQ // KEY_BLOCK, KEY_BLOCK, HEAD_DIM),
        h_all.reshape(TOKENS, MODEL),
        *pooled,
    )
    return run_finish(*outs)


def solution(mesh):
    placed = (
        P(("kv", "tp"), None),
        P("kv", "tp"),
        P("kv", "tp"),
        P("kv", "tp"),
        P(None, "tp", "kv"),
        P(None, "tp", "kv"),
        P("tp", "kv", None),
        P("kv", "tp"),
    )
    return jax.shard_map(
        body,
        mesh=mesh,
        in_specs=placed,
        out_specs=(P("kv", "tp"), P("kv", "tp"), P("kv", "tp"), P("kv", "tp")),
        check_vma=False,
    )
```

time: 152 us -> 150 us (0.987)
  local copies, waits for them, and re-layouts: 9.28 us -> 0.01 us
  Pallas kernels: 142 us -> 150 us
    pallas_call x1, Pallas kernels: 68.7 us -> 90.9 us  [run_scatter(): pl.pallas_call(scatter_kernel, name='scatter', out_shape=(jax.ShapeDtypeS...]
    pallas_call x1 -> x0, Pallas kernels: 14.5 us -> none  [run_chosen(): pl.pallas_call(chosen_kernel, name='chosen', out_shape=(jax.ShapeDtypeStr...]
    unnamed x24 -> x2, local copies, waits for them, and re-layouts: 9.28 us -> 0.01 us
where the time goes in v3:
time: 150 us
  Pallas kernels  150 us (100%)
    pallas_call x1, Pallas kernels, run_scatter(): pl.pallas_call(scatter_kernel, name='scatter', out_shape=(jax.ShapeDtypeS...  90.9 us
    pallas_call x1, Pallas kernels, run_gather(): pl.pallas_call(gather_kernel, name='gather', out_shape=(jax.ShapeDtypeStr...  57.2 us

profile of v3, /device:TPU:0, one launch (start us, length us, event | category | flops | bytes accessed | tf_op | source)
XLA Modules:
  0.0 150.2 jit_solution(1290171901760163276)
XLA Ops:
  0.6 0.0 copy-start
  0.6 57.2 %gather.1 = (bf16[16,1024,128]{2,1,0:T(8,128)(2,1)S(1)}, bf16[16,1024,128]{2,1,0:T(8,128)(2,1)S(1)}, bf16[8,128,4096]{2,1,0:T(8,128)(2,1)S(1)}, f32[8,128,512]{2...) custom-call(bf16[1024,128]{1,0:T(8,128)(2,1)} %k_ref.1, ...), custom_call_target="tpu_custom_call" | custom-call | flops 40000000000 | bytes 8388608 | tf_op jit(solution)/shard_map/gather/pallas_call | solution.py:285
  57.8 0.0 copy-done
  57.8 90.9 %scatter.1 = (bf16[1024,512]{1,0:T(8,128)(2,1)S(1)}, bf16[1024,128]{1,0:T(8,128)(2,1)S(1)}, bf16[1024,128]{1,0:T(8,128)(2,1)S(1)}, f32[256,512]{1,0:T(8,128)S(1)}) custom-call(s32[8,16]{1,0:T(8,128)S(1)} %bitcast.7, bf16[512,32,128]{2,1,0:T(8,128)(2,1)S(1)} %bitcast.5, bf16[512,32,128]{2,1,0:T(8,128)(2,1)S(1)} %bitcast.6, bf16[1024,4096]{1,0:T(8,128)(2,1)S(1)} %bitcast.4, ...), custom_call_target="tpu_custom_call" | custom-call | tf_op jit(solution)/shard_map/scatter/pallas_call | solution.py:586
  148.8 1.4 finish.1
Async XLA Ops:
  0.6 57.2 %copy-start = (s32[1,8,16]{2,1,0:T(8,128)S(1)}, s32[1,8,16]{2,1,0:T(8,128)}, u32[]{:S(2)}) copy-start(s32[1,8,16]{2,1,0:T(8,128)} %param.14) | copy-start | bytes 1540

commit v4 on v3

--- a/solution.py
+++ b/solution.py
@@ -424,16 +424,18 @@
 GW_COLS = MODEL // OWNERS
 PAIR = GROUP // 2 * HEAD_DIM
 PAIR_Q = GROUP // 2 * QUERY_BLOCK
+UNROLL = 4
+HALF_BLOCK = KEY_BLOCK // 2
 SETS = CHOSEN * KEY_BLOCK
 
 
 def scatter_kernel(
     chosen_ref, k_ref, v_ref, h_ref, dqp_ref, dpk_ref, dpv_ref, qs_all, cs_all, ls_rows,
     gq_ref, gk_out, gv_out, gw_out,
-    kb, vb, dk_set, dv_set, gqt, dk_all, dv_all, gw0, gw1, gw2, gw3, order, *rest
+    kb, vb, dk_set, dv_set, gqt, dk0, dv0, dk1, dv1, gw0, gw1, gw2, gw3, *rest
 ):
-    bufs = [rest[i * REDUCE_BUFS : (i + 1) * REDUCE_BUFS] for i in range(6)]
-    send_sems, recv_sems = rest[6 * REDUCE_BUFS :]
+    bufs = [rest[i * REDUCE_BUFS : (i + 1) * REDUCE_BUFS] for i in range(8)]
+    send_sems, recv_sems = rest[8 * REDUCE_BUFS :]
     kv, tp, cz, cy, cx, core = place()
 
     def along(axis, o):
@@ -445,9 +447,10 @@
     greet(peers)
     send = Sender(send_sems, recv_sems)
     gws = (gw0, gw1, gw2, gw3)
-    rk, rv, w0, w1, w2, w3 = [
+    kv_parts = (dk0, dv0, dk1, dv1)
+    k0, v0, k1, v1, w0, w1, w2, w3 = [
         Reduce(send, axis, src, buf, (cz, cy), along)
-        for axis, src, buf in zip((0, 1, 0, 1, 0, 1), (dk_all, dv_all) + gws, bufs)
+        for axis, src, buf in zip((0, 1) * 4, kv_parts + gws, bufs)
     ]
 
     ahead = (
@@ -494,13 +497,16 @@
 
     def product(pair):
         def one(j, carry):
-            cols = pl.ds(pl.multiple_of(j * GW_COLS, GW_COLS), GW_COLS)
+            wide = SIDE * GW_COLS
+            cols = pl.ds(pl.multiple_of(j * wide, wide), wide)
             part = dot(gqt[pair * PAIR : (pair + 1) * PAIR, :], h_ref[:, cols], NN).astype(BF16)
-            gws[2 * pair][j // SIDE, j % SIDE] = part[:HEAD_DIM]
-            gws[2 * pair + 1][j // SIDE, j % SIDE] = part[HEAD_DIM:]
+            for i in range(SIDE):
+                piece = part[:, i * GW_COLS : (i + 1) * GW_COLS]
+                gws[2 * pair][j, i] = piece[:HEAD_DIM]
+                gws[2 * pair + 1][j, i] = piece[HEAD_DIM:]
             return carry
 
-        lax.fori_loop(0, OWNERS, one, 0)
+        lax.fori_loop(0, SIDE, one, 0)
 
     lax.fori_loop(0, BLOCKS, attend(0), 0)
     product(0)
@@ -512,6 +518,12 @@
     w1.combine()
     lax.fori_loop(BLOCKS // 2, BLOCKS, attend(1), 0)
 
+    product(1)
+    w2.begin()
+    w3.begin()
+    w0.turn()
+    w1.turn()
+
     lane = lax.broadcasted_iota(jnp.int32, (1, BLOCKS * CHOSEN), 1)
     listed = jnp.zeros((1, BLOCKS * CHOSEN), jnp.int32)
     for b in range(BLOCKS):
@@ -522,35 +534,32 @@
     hits = jnp.where(hits, 1.0, 0.0).astype(BF16)
     plane = (SIDE, SIDE, POOLED, HEAD_DIM)
 
-    def spread(r, carry):
-        every = pl.ds(r, BLOCKS * CHOSEN, stride=KEY_BLOCK)
-        part = jnp.concatenate([dk_set[every, :], dv_set[every, :]], axis=1).astype(BF16)
-        got = dot(hits, part, NN)
-        rows = pl.ds(pl.multiple_of(r * POOLED, POOLED), POOLED)
-        dk = got[:, :HEAD_DIM] * SCALE + dpk_ref[...]
-        dv = got[:, HEAD_DIM:] + dpv_ref[...]
-        dk_all[:, :, rows, :] = dk.astype(BF16).reshape(plane)
-        dv_all[:, :, rows, :] = dv.astype(BF16).reshape(plane)
-        return carry
-
-    lax.fori_loop(0, KEY_BLOCK, spread, 0)
-    rk.begin()
-    rv.begin()
-    w0.turn()
-    w1.turn()
-    product(1)
-    rk.combine()
-    rv.combine()
-    w2.begin()
-    w3.begin()
+    def spread(part):
+        dk_out, dv_out = kv_parts[2 * part : 2 * part + 2]
+
+        def one(i, carry):
+            every = pl.ds(part * HALF_BLOCK + i, BLOCKS * CHOSEN, stride=KEY_BLOCK)
+            got = jnp.concatenate([dk_set[every, :], dv_set[every, :]], axis=1).astype(BF16)
+            got = dot(hits, got, NN)
+            rows = pl.ds(pl.multiple_of(i * POOLED, POOLED), POOLED)
+            dk = got[:, :HEAD_DIM] * SCALE + dpk_ref[...]
+            dv = got[:, HEAD_DIM:] + dpv_ref[...]
+            dk_out[:, :, rows, :] = dk.astype(BF16).reshape(plane)
+            dv_out[:, :, rows, :] = dv.astype(BF16).reshape(plane)
+            return carry
+
+        lax.fori_loop(0, HALF_BLOCK, one, 0, unroll=UNROLL)
+
+    spread(0)
+    k0.begin()
+    v0.begin()
+    w2.combine()
+    w3.combine()
     w0.combine2()
     w1.combine2()
-    rk.turn()
-    rv.turn()
-    w2.combine()
-    w3.combine()
-    rk.combine2()
-    rv.combine2()
+    spread(1)
+    k1.begin()
+    v1.begin()
     w2.turn()
     w3.turn()
 
@@ -559,29 +568,47 @@
             at = n * HEAD_DIM + i * HEAD_DIM // 2
             gw_out[:, at : at + HEAD_DIM // 2] = part.T
 
+    def ordered(into, part, r):
+        for n, rows in enumerate(r.end()):
+            for i in range(HALF_BLOCK // 2):
+                at = part * HALF_BLOCK + n * (HALF_BLOCK // 2) + i
+                into[pl.ds(at, POOLED, stride=KEY_BLOCK), :] = rows[i * POOLED : (i + 1) * POOLED]
+
     weight(0, w0)
     weight(1, w1)
-    for r, out in ((rk, gk_out), (rv, gv_out)):
-        for n, part in enumerate(r.end()):
-            for i in range(KEY_BLOCK // 2):
-                at = n * (KEY_BLOCK // 2) + i
-                order[pl.ds(at, POOLED, stride=KEY_BLOCK), :] = part[i * POOLED : (i + 1) * POOLED]
-        out[...] = order[...].astype(BF16)
+    k0.combine()
+    v0.combine()
     w2.combine2()
     w3.combine2()
+    k1.combine()
+    v1.combine()
     weight(2, w2)
     weight(3, w3)
+    k0.turn()
+    v0.turn()
+    k1.turn()
+    v1.turn()
+    k0.combine2()
+    v0.combine2()
+    k1.combine2()
+    v1.combine2()
+    ordered(dk_set, 0, k0)
+    ordered(dv_set, 0, v0)
+    ordered(dk_set, 1, k1)
+    ordered(dv_set, 1, v1)
+    gk_out[...] = dk_set[:TOKENS, :].astype(BF16)
+    gv_out[...] = dv_set[:TOKENS, :].astype(BF16)
     send.finish()
 
 
-SCATTER_COPIES = 6 * 12
-SCATTER_MIB = 31
+SCATTER_COPIES = 8 * 12
+SCATTER_MIB = 30.7
 
 
 def run_scatter(chosen, k_all, v_all, h_all, dqp, dpk, dpv, qs, cs, ls):
     vmem = pl.BlockSpec(memory_space=pltpu.VMEM)
     smem = pl.BlockSpec(memory_space=pltpu.SMEM)
-    dense = pltpu.VMEM((SIDE, SIDE, TOKENS, HEAD_DIM), BF16)
+    dense = pltpu.VMEM((SIDE, SIDE, TOKENS // 2, HEAD_DIM), BF16)
     grad = pltpu.VMEM((SIDE, SIDE, HEAD_DIM, GW_COLS), BF16)
     return pl.pallas_call(
         scatter_kernel,
@@ -602,19 +629,19 @@
             pltpu.VMEM((GROUP * HEAD_DIM, TOKENS), BF16),
             dense,
             dense,
+            dense,
+            dense,
             grad,
             grad,
             grad,
             grad,
-            pltpu.VMEM((TOKENS, HEAD_DIM), F32),
-            *reduce_buffers(TOKENS, HEAD_DIM),
-            *reduce_buffers(TOKENS, HEAD_DIM),
+            *(reduce_buffers(TOKENS // 2, HEAD_DIM) * 4),
             *(reduce_buffers(HEAD_DIM, GW_COLS) * 4),
             pltpu.SemaphoreType.DMA((SCATTER_COPIES,)),
             pltpu.SemaphoreType.DMA((SCATTER_COPIES,)),
         ],
         compiler_params=pltpu.CompilerParams(
-            collective_id=1, has_side_effects=True, vmem_limit_bytes=SCATTER_MIB * MIB
+            collective_id=1, has_side_effects=True, vmem_limit_bytes=int(SCATTER_MIB * MIB)
         ),
     )(chosen, k_all, v_all, h_all, dqp, dpk, dpv, qs, cs, ls)
 

time: 150 us -> 140 us (0.933)
  Pallas kernels: 150 us -> 139 us
    pallas_call x1, Pallas kernels: 90.9 us -> 80.6 us  [run_scatter(): pl.pallas_call(scatter_kernel, name='scatter', out_shape=(jax.ShapeDtypeS...]
where the time goes in v4:
time: 140 us
  Pallas kernels  139 us (99%)
    pallas_call x1, Pallas kernels, run_scatter(): pl.pallas_call(scatter_kernel, name='scatter', out_shape=(jax.ShapeDtypeS...  80.6 us
    pallas_call x1, Pallas kernels, run_gather(): pl.pallas_call(gather_kernel, name='gather', out_shape=(jax.ShapeDtypeStr...  57.2 us

profile of v4, /device:TPU:0, one launch (start us, length us, event | category | flops | bytes accessed | tf_op | source)
XLA Modules:
  0.0 139.9 jit_solution(4943721261845641045)
XLA Ops:
  0.6 0.0 copy-start
  0.6 57.2 %gather.1 = (bf16[16,1024,128]{2,1,0:T(8,128)(2,1)S(1)}, bf16[16,1024,128]{2,1,0:T(8,128)(2,1)S(1)}, bf16[8,128,4096]{2,1,0:T(8,128)(2,1)S(1)}, f32[8,128,512]{2...) custom-call(bf16[1024,128]{1,0:T(8,128)(2,1)} %k_ref.1, ...), custom_call_target="tpu_custom_call" | custom-call | flops 40000000000 | bytes 8388608 | tf_op jit(solution)/shard_map/gather/pallas_call | solution.py:285
  57.8 0.0 copy-done
  57.8 80.6 %scatter.1 = (bf16[1024,512]{1,0:T(8,128)(2,1)S(1)}, bf16[1024,128]{1,0:T(8,128)(2,1)S(1)}, bf16[1024,128]{1,0:T(8,128)(2,1)S(1)}, f32[256,512]{1,0:T(8,128)S(1)}) custom-call(s32[8,16]{1,0:T(8,128)S(1)} %bitcast.7, bf16[512,32,128]{2,1,0:T(8,128)(2,1)S(1)} %bitcast.5, bf16[512,32,128]{2,1,0:T(8,128)(2,1)S(1)} %bitcast.6, bf16[1024,4096]{1,0:T(8,128)(2,1)S(1)} %bitcast.4, ...), custom_call_target="tpu_custom_call" | custom-call | tf_op jit(solution)/shard_map/scatter/pallas_call | solution.py:613
  138.4 1.4 %finish.1 = (bf16[1024,512]{1,0:T(8,128)(2,1)}, bf16[1024,128]{1,0:T(8,128)(2,1)}, bf16[1024,128]{1,0:T(8,128)(2,1)}, f32[256,512]{1,0:T(8,128)}) custom-call(bf16[1024,512]{1,0:T(8,128)(2,1)S(1)} %get-tuple-element.26.refs_0_, bf16[1024,128]{1,0:T(8,128)(2,1)S(1)} %get-tuple-element.27.refs_1_, bf16[1024,128]{1,0:T(8,128)(2,1)S(1)} %get-tuple-element.28.refs_2_, ...), custom_call_target="tpu_custom_call" | custom-call | tf_op jit(solution)/shard_map/finish/pallas_call | solution.py:656
Async XLA Ops:
  0.6 57.2 %copy-start = (s32[1,8,16]{2,1,0:T(8,128)S(1)}, s32[1,8,16]{2,1,0:T(8,128)}, u32[]{:S(2)}) copy-start(s32[1,8,16]{2,1,0:T(8,128)} %param.14) | copy-start | bytes 1540

commit v5 on v4

--- a/solution.py
+++ b/solution.py
@@ -19,6 +19,8 @@
 BLOCKS = TOKENS // QUERY_BLOCK
 POOLED = TOKENS // POOL_BLOCK
 SEQ = TOKENS * OWNERS
+LISTED = BLOCKS * CHOSEN
+SLOTS = OWNERS * CHOSEN
 MODEL = 4096
 SCALE = HEAD_DIM ** (-0.5)
 LOG2E = 1.4426950408889634
@@ -108,9 +110,9 @@
 
 
 def gather_kernel(
-    k_ref, v_ref, h_ref, q_hbm, g_hbm, gate_hbm, ls_hbm,
-    k_all, v_all, h_all, dq_ref, dpk_ref, dpv_ref, qs_all, cs_all, ls_rows,
-    q_ref, g_ref, gate_ref, ls_ref, pool_all, pk_ref, pv_ref, pool_here,
+    k_ref, v_ref, h_ref, q_hbm, g_hbm, gate_hbm, ls_hbm, chosen_hbm,
+    k_all, v_all, h_all, dq_ref, dpk_ref, dpv_ref, qs_all, cs_all, ls_rows, pick_ref, place_ref,
+    chosen_ref, q_ref, g_ref, gate_ref, ls_ref, pool_all, pk_ref, pv_ref, pool_here,
     pool_send, pool_recv, send_sems, recv_sems, local_sems,
 ):
     kv, tp, cz, cy, cx, core = place()
@@ -141,6 +143,7 @@
                 (k_ref, k_all.at[kv]),
                 (v_ref, v_all.at[kv]),
                 (h_ref, h_all.at[tp]),
+                (chosen_hbm, chosen_ref),
                 (gate_hbm, gate_ref),
                 (ls_hbm, ls_ref),
                 (q_hbm, q_ref),
@@ -158,6 +161,16 @@
     pool_here[0] = dot(mean, k_all[kv], NN).astype(BF16)
     local[1].wait()
     pool_here[1] = dot(mean, v_all[kv], NN).astype(BF16)
+
+    local[3].wait()
+    lane = lax.broadcasted_iota(jnp.int32, (1, LISTED), 1)
+    listed = jnp.zeros((1, LISTED), jnp.int32)
+    for b in range(BLOCKS):
+        for c in range(CHOSEN):
+            listed = jnp.where(lane == b * CHOSEN + c, chosen_ref[b, c], listed)
+    row = lax.broadcasted_iota(jnp.int32, (POOLED, LISTED), 0)
+    both = jnp.where(row == 0, listed // POOLED, jnp.where(row == 1, listed % POOLED, 0))
+    pool_here[2] = both.astype(F32).astype(BF16)
     meet(len(peers))
 
     pool_sender = Sender(pool_send, pool_recv)
@@ -179,7 +192,7 @@
         here = full.at[kv]
         wide[axis] = [(0, [send(here, here, along(1 - axis, s)) for s in (1, -1)])]
 
-    for copy in local[3:]:
+    for copy in local[4:]:
         copy.wait()
     for copy in pool_sender.sent:
         copy.wait_recv()
@@ -187,6 +200,49 @@
     pv_ref[...] = pool_all[:, 1].reshape(OWNERS * POOLED, HEAD_DIM)
     dpk_ref[...] = jnp.zeros_like(dpk_ref)
     dpv_ref[...] = jnp.zeros_like(dpv_ref)
+
+    def listing(i):
+        both = pool_all[i, 2].astype(F32)
+        owners, numbers, column = both[0:1, :], both[1:2, :], both.T[:, 0:1]
+        one = lax.broadcasted_iota(jnp.int32, (LISTED, LISTED), 0)
+        two = lax.broadcasted_iota(jnp.int32, (LISTED, LISTED), 1)
+        same = jnp.where(column == owners, 1.0, 0.0)
+        rank = jnp.sum(jnp.where(one < two, same, 0.0), axis=0, keepdims=True)
+        return owners, numbers, rank
+
+    def grid(rows, f):
+        return f(lax.broadcasted_iota(jnp.int32, (rows, LISTED), 0)).astype(F32)
+
+    def ones(seen):
+        return jnp.where(seen, 1.0, 0.0)
+
+    owners, numbers, rank = listing(kv)
+    kv_f = kv.astype(F32)
+    at, nth = grid(SLOTS, lambda i: i // CHOSEN), grid(SLOTS, lambda i: i % CHOSEN)
+    own = jnp.where(owners == kv_f, -1.0, owners)
+    pick_ref[:SLOTS] = (ones(own == at) * ones(rank == nth)).astype(BF16)
+    at = grid(POOLED, lambda i: i)
+    pick_ref[SLOTS:] = (ones(owners == kv_f) * ones(numbers == at)).astype(BF16)
+
+    for axis in (0, 1):
+        def owner_id(i, axis=axis):
+            return cz * SIDE + i if axis == 0 else i * SIDE + cy
+
+        for pair in (0, 1):
+            total = None
+            for n in (0, 1):
+                who = owner(axis, (0, -1, 1, 2)[2 * pair + n], 0)
+                owners, numbers, rank = listing(who)
+                at = grid(LISTED, lambda i: owner_id(i // POOLED))
+                nth = grid(LISTED, lambda i: i % POOLED)
+                blocks = ones(owners == at) * ones(numbers == nth)
+                at = grid(LISTED, lambda i: owner_id((i % 64) // CHOSEN))
+                nth = grid(LISTED, lambda i, n=n: jnp.where(i // 64 == n, i % CHOSEN, -1))
+                own = jnp.where(owners == who.astype(F32), -1.0, owners)
+                slots = ones(own == at) * ones(rank == nth)
+                part = dot(blocks.astype(BF16), slots.astype(BF16), NT)
+                total = part if total is None else total + part
+            place_ref[axis, :, pair * LISTED : (pair + 1) * LISTED] = total.astype(BF16)
 
     n_pool = OWNERS * POOLED
     wide_q = GROUP * QUERY_BLOCK
@@ -277,7 +333,7 @@
 GATHER_COPIES = 2 * (2 + 2 + 8 + 8) + 2 + 2 + 4
 
 
-def run_gather(k, v, h, q, g, gates, sums):
+def run_gather(k, v, h, q, g, gates, sums, chosen):
     hbm = pl.BlockSpec(memory_space=pltpu.HBM)
     vmem = pl.BlockSpec(memory_space=pltpu.VMEM)
     n_pool = OWNERS * POOLED
@@ -295,23 +351,26 @@
             jax.ShapeDtypeStruct((BLOCKS, wide_q, HEAD_DIM), BF16),
             jax.ShapeDtypeStruct((BLOCKS, wide_q, HEAD_DIM), BF16),
             jax.ShapeDtypeStruct((BLOCKS, 1, wide_q), F32),
+            jax.ShapeDtypeStruct((SLOTS + POOLED, LISTED), BF16),
+            jax.ShapeDtypeStruct((2, LISTED, SLOTS), BF16),
         ),
-        in_specs=[hbm] * 7,
-        out_specs=(vmem,) * 9,
+        in_specs=[hbm] * 8,
+        out_specs=(vmem,) * 11,
         scratch_shapes=[
+            pltpu.SMEM((BLOCKS, CHOSEN), jnp.int32),
             pltpu.VMEM(q.shape, BF16),
             pltpu.VMEM(g.shape, BF16),
             pltpu.VMEM(gates.shape, F32),
             pltpu.VMEM(sums.shape, F32),
-            pltpu.VMEM((OWNERS, 2, POOLED, HEAD_DIM), BF16),
+            pltpu.VMEM((OWNERS, 3, POOLED, HEAD_DIM), BF16),
             pltpu.VMEM((n_pool, HEAD_DIM), BF16),
             pltpu.VMEM((n_pool, HEAD_DIM), BF16),
-            pltpu.VMEM((2, POOLED, HEAD_DIM), BF16),
+            pltpu.VMEM((3, POOLED, HEAD_DIM), BF16),
             pltpu.SemaphoreType.DMA((OWNERS - 1,)),
             pltpu.SemaphoreType.DMA((OWNERS - 1,)),
             pltpu.SemaphoreType.DMA((GATHER_COPIES,)),
             pltpu.SemaphoreType.DMA((GATHER_COPIES,)),
-            pltpu.SemaphoreType.DMA((7,)),
+            pltpu.SemaphoreType.DMA((8,)),
         ],
         compiler_params=pltpu.CompilerParams(
             collective_id=0, has_side_effects=True, vmem_limit_bytes=12 * MIB
@@ -319,7 +378,7 @@
         cost_estimate=pl.CostEstimate(
             flops=40_000_000_000, bytes_accessed=8 * MIB, transcendentals=0
         ),
-    )(*(pltpu.with_memory_space_constraint(a, pltpu.HBM) for a in (k, v, h, q, g, gates, sums)))
+    )(*(pltpu.with_memory_space_constraint(a, pltpu.HBM) for a in (k, v, h, q, g, gates, sums, chosen)))
 
 
 class Reduce:
@@ -383,6 +442,9 @@
             return carry
 
         lax.fori_loop(0, SIDE, add, 0)
+        self.start_second()
+
+    def start_second(self):
         s = self.send
         self.r = [
             s(self.part(2, 0), self.relay2.at[0], self.to2(1)),
@@ -413,6 +475,83 @@
         ]
 
 
+class ListedReduce(Reduce):
+    def __init__(self, send, axis, src, bufs, coords, along, place_ref, own):
+        self.passed, self.far, self.near, *after = bufs
+        super().__init__(send, axis, src, (None, None, *after), coords, along)
+        self.place_ref, self.own = place_ref, own
+        self.steps = HALF_BLOCK * CHOSEN
+        self.pooled = self
+
+    def begin(self):
+        s = self.send
+        every = pl.ds(0, self.src.shape[2])
+        self.rows = self.rows + (every,)
+        self.r = [
+            s(self.bundle(2, 0), self.passed.at[0], self.to1(1)),
+            s(self.bundle(2, 1), self.passed.at[1], self.to1(-1)),
+        ]
+        self.d = [
+            s(self.bundle(1, 2), self.near.at[0], self.to1(1)),
+            s(self.bundle(-1, 2), self.near.at[1], self.to1(-1)),
+        ]
+
+    def combine(self):
+        self.c = []
+        for n, o in enumerate((1, -1)):
+            self.r[n].wait_recv()
+            self.c.append(self.send(self.passed.at[n], self.far.at[:, self.rows[n]], self.to1(o)))
+
+    def sources(self, rows):
+        mine = self.src[self.c1, :, rows, :] if self.axis == 0 else self.src[:, self.c1, rows, :]
+        return [mine, self.near[0, :, rows, :], self.near[1, :, rows, :], self.far[:, rows, :]]
+
+    def turn(self):
+        for copy in self.d + self.c:
+            copy.wait_recv()
+        pooled = sum(x.astype(F32) for x in self.pooled.sources(pl.ds(self.steps, POOLED)))
+        pooled = pooled.reshape(SIDE * POOLED, HEAD_DIM)
+        pooled = jnp.concatenate([pooled, pooled], axis=1)
+        for n in (0, 1):
+
+            def put(i, carry, n=n):
+                pieces = []
+                for j in (0, 1):
+                    first = pl.multiple_of((n * HALF_BLOCK // 2 + 2 * i + j) * CHOSEN, CHOSEN)
+                    got = [x.reshape(SIDE * CHOSEN, HEAD_DIM) for x in self.sources(pl.ds(first, CHOSEN))]
+                    pieces.append(jnp.concatenate(got, axis=0))
+                total = dot(self.place_ref[self.axis], jnp.concatenate(pieces, axis=1), NN)
+                total = total + pooled
+                for j in (0, 1):
+                    rows = pl.ds(pl.multiple_of((2 * i + j) * POOLED, POOLED), POOLED)
+                    part = total[:, j * HEAD_DIM : (j + 1) * HEAD_DIM].astype(BF16)
+                    self.comb[n, :, rows, :] = part.reshape(SIDE, POOLED, HEAD_DIM)
+                return carry
+
+            lax.fori_loop(0, HALF_BLOCK // 4, put, 0, unroll=2)
+        self.start_second()
+
+    def end(self):
+        at = self.own[1]
+        size = HALF_BLOCK // 2 * POOLED
+        return [
+            part + self.own[0][at + n * size : at + (n + 1) * size, :]
+            for n, part in enumerate(super().end())
+        ]
+
+
+def listed_buffers(rows):
+    half, size = rows // 2, HALF_BLOCK // 2 * POOLED
+    slim = pltpu.VMEM((2, size, HEAD_DIM), BF16)
+    return [
+        pltpu.VMEM((2, SIDE, half, HEAD_DIM), BF16),
+        pltpu.VMEM((SIDE, rows, HEAD_DIM), BF16),
+        pltpu.VMEM((2, SIDE, rows, HEAD_DIM), BF16),
+        pltpu.VMEM((2, SIDE, size, HEAD_DIM), BF16),
+        slim, slim, slim,
+    ]
+
+
 def reduce_buffers(rows, lanes):
     half = rows // 2
     wide = pltpu.VMEM((2, SIDE, half, lanes), BF16)
@@ -421,6 +560,7 @@
 
 
 REDUCE_BUFS = 6
+LISTED_BUFS = 7
 GW_COLS = MODEL // OWNERS
 PAIR = GROUP // 2 * HEAD_DIM
 PAIR_Q = GROUP // 2 * QUERY_BLOCK
@@ -430,12 +570,14 @@
 
 
 def scatter_kernel(
-    chosen_ref, k_ref, v_ref, h_ref, dqp_ref, dpk_ref, dpv_ref, qs_all, cs_all, ls_rows,
+    chosen_ref, k_ref, v_ref, h_ref, dqp_ref, dpk_ref, dpv_ref, qs_all, cs_all, ls_rows, pick_ref, place_ref,
     gq_ref, gk_out, gv_out, gw_out,
-    kb, vb, dk_set, dv_set, gqt, dk0, dv0, dk1, dv1, gw0, gw1, gw2, gw3, *rest
+    kb, vb, dk_set, dv_set, gqt, dk0, dv0, dk1, dv1, own_k, own_v, gw0, gw1, gw2, gw3, *rest
 ):
-    bufs = [rest[i * REDUCE_BUFS : (i + 1) * REDUCE_BUFS] for i in range(8)]
-    send_sems, recv_sems = rest[8 * REDUCE_BUFS :]
+    cut = 4 * LISTED_BUFS
+    bufs = [rest[i * LISTED_BUFS : (i + 1) * LISTED_BUFS] for i in range(4)]
+    gw_bufs = [rest[cut + i * REDUCE_BUFS : cut + (i + 1) * REDUCE_BUFS] for i in range(4)]
+    send_sems, recv_sems = rest[cut + 4 * REDUCE_BUFS :]
     kv, tp, cz, cy, cx, core = place()
 
     def along(axis, o):
@@ -448,9 +590,16 @@
     send = Sender(send_sems, recv_sems)
     gws = (gw0, gw1, gw2, gw3)
     kv_parts = (dk0, dv0, dk1, dv1)
-    k0, v0, k1, v1, w0, w1, w2, w3 = [
+    half_rows = HALF_BLOCK * POOLED
+    owns = ((own_k, 0), (own_v, 0), (own_k, half_rows), (own_v, half_rows))
+    k0, v0, k1, v1 = [
+        ListedReduce(send, axis, src, buf, (cz, cy), along, place_ref, own)
+        for axis, src, buf, own in zip((0, 1) * 2, kv_parts, bufs, owns)
+    ]
+    k1.pooled, v1.pooled = k0, v0
+    w0, w1, w2, w3 = [
         Reduce(send, axis, src, buf, (cz, cy), along)
-        for axis, src, buf in zip((0, 1) * 4, kv_parts + gws, bufs)
+        for axis, src, buf in zip((0, 1) * 2, gws, gw_bufs)
     ]
 
     ahead = (
@@ -486,10 +635,10 @@
                 gq_ref[rows, at : at + HEAD_DIM] = part.T.astype(BF16)
             here = pl.ds(pl.multiple_of(b * SETS, SETS), SETS)
             if pair == 0:
-                dk_set[here, :] = dk
+                dk_set[here, :] = dk * SCALE
                 dv_set[here, :] = dv
             else:
-                dk_set[here, :] += dk
+                dk_set[here, :] += dk * SCALE
                 dv_set[here, :] += dv
             return carry
 
@@ -524,32 +673,29 @@
     w0.turn()
     w1.turn()
 
-    lane = lax.broadcasted_iota(jnp.int32, (1, BLOCKS * CHOSEN), 1)
-    listed = jnp.zeros((1, BLOCKS * CHOSEN), jnp.int32)
-    for b in range(BLOCKS):
-        for c in range(CHOSEN):
-            listed = jnp.where(lane == b * CHOSEN + c, chosen_ref[b, c], listed)
-    n_pool = OWNERS * POOLED
-    hits = lax.broadcasted_iota(jnp.int32, (n_pool, BLOCKS * CHOSEN), 0) == listed
-    hits = jnp.where(hits, 1.0, 0.0).astype(BF16)
-    plane = (SIDE, SIDE, POOLED, HEAD_DIM)
+    slots = (SIDE, SIDE, CHOSEN, HEAD_DIM)
 
     def spread(part):
         dk_out, dv_out = kv_parts[2 * part : 2 * part + 2]
 
         def one(i, carry):
-            every = pl.ds(part * HALF_BLOCK + i, BLOCKS * CHOSEN, stride=KEY_BLOCK)
+            every = pl.ds(part * HALF_BLOCK + i, LISTED, stride=KEY_BLOCK)
             got = jnp.concatenate([dk_set[every, :], dv_set[every, :]], axis=1).astype(BF16)
-            got = dot(hits, got, NN)
-            rows = pl.ds(pl.multiple_of(i * POOLED, POOLED), POOLED)
-            dk = got[:, :HEAD_DIM] * SCALE + dpk_ref[...]
-            dv = got[:, HEAD_DIM:] + dpv_ref[...]
-            dk_out[:, :, rows, :] = dk.astype(BF16).reshape(plane)
-            dv_out[:, :, rows, :] = dv.astype(BF16).reshape(plane)
+            got = dot(pick_ref[...], got, NN)
+            rows = pl.ds(pl.multiple_of(i * CHOSEN, CHOSEN), CHOSEN)
+            dk_out[:, :, rows, :] = got[:SLOTS, :HEAD_DIM].astype(BF16).reshape(slots)
+            dv_out[:, :, rows, :] = got[:SLOTS, HEAD_DIM:].astype(BF16).reshape(slots)
+            rows = pl.ds(pl.multiple_of((part * HALF_BLOCK + i) * POOLED, POOLED), POOLED)
+            own_k[rows, :] = got[SLOTS:, :HEAD_DIM]
+            own_v[rows, :] = got[SLOTS:, HEAD_DIM:]
             return carry
 
         lax.fori_loop(0, HALF_BLOCK, one, 0, unroll=UNROLL)
 
+    tail = slice(HALF_BLOCK * CHOSEN, HALF_BLOCK * CHOSEN + POOLED)
+    pooled = (SIDE, SIDE, POOLED, HEAD_DIM)
+    dk0[:, :, tail, :] = dpk_ref[...].astype(BF16).reshape(pooled)
+    dv0[:, :, tail, :] = dpv_ref[...].astype(BF16).reshape(pooled)
     spread(0)
     k0.begin()
     v0.begin()
@@ -602,13 +748,15 @@
 
 
 SCATTER_COPIES = 8 * 12
-SCATTER_MIB = 30.7
-
-
-def run_scatter(chosen, k_all, v_all, h_all, dqp, dpk, dpv, qs, cs, ls):
+SCATTER_MIB = 28
+
+
+def run_scatter(chosen, k_all, v_all, h_all, dqp, dpk, dpv, qs, cs, ls, pick, places):
     vmem = pl.BlockSpec(memory_space=pltpu.VMEM)
     smem = pl.BlockSpec(memory_space=pltpu.SMEM)
-    dense = pltpu.VMEM((SIDE, SIDE, TOKENS // 2, HEAD_DIM), BF16)
+    first = HALF_BLOCK * CHOSEN + POOLED
+    second = HALF_BLOCK * CHOSEN
+    outgoing = [pltpu.VMEM((SIDE, SIDE, n, HEAD_DIM), BF16) for n in (first, first, second, second)]
     grad = pltpu.VMEM((SIDE, SIDE, HEAD_DIM, GW_COLS), BF16)
     return pl.pallas_call(
         scatter_kernel,
@@ -619,7 +767,7 @@
             jax.ShapeDtypeStruct((TOKENS, HEAD_DIM), BF16),
             jax.ShapeDtypeStruct((GW_COLS, GROUP * HEAD_DIM), F32),
         ),
-        in_specs=[smem] + [vmem] * 9,
+        in_specs=[smem] + [vmem] * 11,
         out_specs=(vmem,) * 4,
         scratch_shapes=[
             pltpu.VMEM((SETS, HEAD_DIM), BF16),
@@ -627,23 +775,23 @@
             pltpu.VMEM((BLOCKS * SETS, HEAD_DIM), F32),
             pltpu.VMEM((BLOCKS * SETS, HEAD_DIM), F32),
             pltpu.VMEM((GROUP * HEAD_DIM, TOKENS), BF16),
-            dense,
-            dense,
-            dense,
-            dense,
+            *outgoing,
+            pltpu.VMEM((TOKENS, HEAD_DIM), F32),
+            pltpu.VMEM((TOKENS, HEAD_DIM), F32),
             grad,
             grad,
             grad,
             grad,
-            *(reduce_buffers(TOKENS // 2, HEAD_DIM) * 4),
+            *(listed_buffers(first) * 2),
+            *(listed_buffers(second) * 2),
             *(reduce_buffers(HEAD_DIM, GW_COLS) * 4),
             pltpu.SemaphoreType.DMA((SCATTER_COPIES,)),
             pltpu.SemaphoreType.DMA((SCATTER_COPIES,)),
         ],
         compiler_params=pltpu.CompilerParams(
-            collective_id=1, has_side_effects=True, vmem_limit_bytes=int(SCATTER_MIB * MIB)
+            collective_id=1, has_side_effects=True, vmem_limit_bytes=SCATTER_MIB * MIB
         ),
-    )(chosen, k_all, v_all, h_all, dqp, dpk, dpv, qs, cs, ls)
+    )(chosen, k_all, v_all, h_all, dqp, dpk, dpv, qs, cs, ls, pick, places)
 
 
 def finish_kernel(*refs):
@@ -664,15 +812,17 @@
 
 
 def body(hidden_rows, queries, key_rows, value_rows, branch_gates, log_sums, chosen, out_grad):
-    k_all, v_all, h_all, *pooled = run_gather(
-        key_rows, value_rows, hidden_rows, queries, out_grad, branch_gates, log_sums
+    lists = chosen.reshape(BLOCKS, CHOSEN)
+    k_all, v_all, h_all, *more = run_gather(
+        key_rows, value_rows, hidden_rows, queries, out_grad, branch_gates, log_sums, lists
     )
+    by_block = (SEQ // KEY_BLOCK, KEY_BLOCK, HEAD_DIM)
     outs = run_scatter(
-        chosen.reshape(BLOCKS, CHOSEN),
-        k_all.reshape(SEQ // KEY_BLOCK, KEY_BLOCK, HEAD_DIM),
-        v_all.reshape(SEQ // KEY_BLOCK, KEY_BLOCK, HEAD_DIM),
+        lists,
+        k_all.reshape(by_block),
+        v_all.reshape(by_block),
         h_all.reshape(TOKENS, MODEL),
-        *pooled,
+        *more,
     )
     return run_finish(*outs)
 

time: 140 us -> 131 us (0.936)
  Pallas kernels: 139 us -> 130 us
    pallas_call x1, Pallas kernels: 80.6 us -> 70.1 us  [run_scatter(): pl.pallas_call(scatter_kernel, name='scatter', out_shape=(jax.ShapeDtypeS...]
    pallas_call x1, Pallas kernels: 57.2 us -> 58.6 us  [run_gather(): pl.pallas_call(gather_kernel, name='gather', out_shape=(jax.ShapeDtypeStr...]
where the time goes in v5:
time: 131 us
  Pallas kernels  130 us (99%)
    pallas_call x1, Pallas kernels, run_scatter(): pl.pallas_call(scatter_kernel, name='scatter', out_shape=(jax.ShapeDtypeS...  70.1 us
    pallas_call x1, Pallas kernels, run_gather(): pl.pallas_call(gather_kernel, name='gather', out_shape=(jax.ShapeDtypeStr...  58.6 us

profile of v5, /device:TPU:0, one launch (start us, length us, event | category | flops | bytes accessed | tf_op | source)
XLA Modules:
  0.0 130.8 jit_solution(12415275388166952520)
XLA Ops:
  0.6 0.0 copy-start
  0.6 58.6 %gather.1 = (bf16[16,1024,128]{2,1,0:T(8,128)(2,1)S(1)}, bf16[16,1024,128]{2,1,0:T(8,128)(2,1)S(1)}, bf16[8,128,4096]{2,1,0:T(8,128)(2,1)S(1)}, f32[8,128,512]{2...) custom-call(bf16[1024,128]{1,0:T(8,128)(2,1)} %k_ref.1, ...), custom_call_target="tpu_custom_call" | custom-call | flops 40000000000 | bytes 8388608 | tf_op jit(solution)/shard_map/gather/pallas_call | solution.py:341
  59.3 0.0 copy-done
  59.3 70.1 %scatter.1 = (bf16[1024,512]{1,0:T(8,128)(2,1)S(1)}, bf16[1024,128]{1,0:T(8,128)(2,1)S(1)}, bf16[1024,128]{1,0:T(8,128)(2,1)S(1)}, f32[256,512]{1,0:T(8,128)S(1)}) custom-call(s32[8,16]{1,0:T(8,128)S(1)} %bitcast.8, bf16[512,32,128]{2,1,0:T(8,128)(2,1)S(1)} %bitcast.5, bf16[512,32,128]{2,1,0:T(8,128)(2,1)S(1)} %bitcast.6, bf16[1024,4096]{1,0:T(8,128)(2,1)S(1)} %bitcast.4, ...), custom_call_target="tpu_custom_call" | custom-call | tf_op jit(solution)/shard_map/scatter/pallas_call | solution.py:761
  129.4 1.4 %finish.1 = (bf16[1024,512]{1,0:T(8,128)(2,1)}, bf16[1024,128]{1,0:T(8,128)(2,1)}, bf16[1024,128]{1,0:T(8,128)(2,1)}, f32[256,512]{1,0:T(8,128)}) custom-call(bf16[1024,512]{1,0:T(8,128)(2,1)S(1)} %get-tuple-element.30.refs_0_, bf16[1024,128]{1,0:T(8,128)(2,1)S(1)} %get-tuple-element.31.refs_1_, bf16[1024,128]{1,0:T(8,128)(2,1)S(1)} %get-tuple-element.32.refs_2_, ...), custom_call_target="tpu_custom_call" | custom-call | tf_op jit(solution)/shard_map/finish/pallas_call | solution.py:804
Async XLA Ops:
  0.6 58.6 %copy-start = (s32[1,8,16]{2,1,0:T(8,128)S(1)}, s32[1,8,16]{2,1,0:T(8,128)}, u32[]{:S(2)}) copy-start(s32[1,8,16]{2,1,0:T(8,128)} %param.14) | copy-start | bytes 1540

commit v6 on v5

--- a/solution.py
+++ b/solution.py
@@ -104,7 +104,7 @@
     p = jnp.where(visible, jnp.exp2(scores - log_sum), 0.0)
     pr = p.astype(BF16)
     dp = dot(values, cs, NT)
-    delta = jnp.sum(pr.astype(F32) * dp, axis=0, keepdims=True)
+    delta = jnp.sum(p * dp, axis=0, keepdims=True)
     ds = (p * (dp - delta)).astype(BF16)
     return dot(keys.T, ds, NN), dot(ds, qs, NN), dot(pr, cs, NN)
 
@@ -158,9 +158,9 @@
     row = lax.broadcasted_iota(jnp.int32, (POOLED, TOKENS), 1)
     mean = jnp.where(row // POOL_BLOCK == blk, 1.0 / POOL_BLOCK, 0.0).astype(BF16)
     local[0].wait()
-    pool_here[0] = dot(mean, k_all[kv], NN).astype(BF16)
+    pool_here[:POOLED] = dot(mean, k_all[kv], NN).astype(BF16)
     local[1].wait()
-    pool_here[1] = dot(mean, v_all[kv], NN).astype(BF16)
+    pool_here[POOLED : POOLED * 2] = dot(mean, v_all[kv], NN).astype(BF16)
 
     local[3].wait()
     lane = lax.broadcasted_iota(jnp.int32, (1, LISTED), 1)
@@ -168,9 +168,9 @@
     for b in range(BLOCKS):
         for c in range(CHOSEN):
             listed = jnp.where(lane == b * CHOSEN + c, chosen_ref[b, c], listed)
-    row = lax.broadcasted_iota(jnp.int32, (POOLED, LISTED), 0)
+    row = lax.broadcasted_iota(jnp.int32, (16, LISTED), 0)
     both = jnp.where(row == 0, listed // POOLED, jnp.where(row == 1, listed % POOLED, 0))
-    pool_here[2] = both.astype(F32).astype(BF16)
+    pool_here[POOLED * 2 :] = both.astype(F32).astype(BF16)
     meet(len(peers))
 
     pool_sender = Sender(pool_send, pool_recv)
@@ -196,13 +196,13 @@
         copy.wait()
     for copy in pool_sender.sent:
         copy.wait_recv()
-    pk_ref[...] = pool_all[:, 0].reshape(OWNERS * POOLED, HEAD_DIM)
-    pv_ref[...] = pool_all[:, 1].reshape(OWNERS * POOLED, HEAD_DIM)
+    pk_ref[...] = pool_all[:, :POOLED].reshape(OWNERS * POOLED, HEAD_DIM)
+    pv_ref[...] = pool_all[:, POOLED : 2 * POOLED].reshape(OWNERS * POOLED, HEAD_DIM)
     dpk_ref[...] = jnp.zeros_like(dpk_ref)
     dpv_ref[...] = jnp.zeros_like(dpv_ref)
 
     def listing(i):
-        both = pool_all[i, 2].astype(F32)
+        both = pool_all[i, 2 * POOLED :].astype(F32)
         owners, numbers, column = both[0:1, :], both[1:2, :], both.T[:, 0:1]
         one = lax.broadcasted_iota(jnp.int32, (LISTED, LISTED), 0)
         two = lax.broadcasted_iota(jnp.int32, (LISTED, LISTED), 1)
@@ -362,10 +362,10 @@
             pltpu.VMEM(g.shape, BF16),
             pltpu.VMEM(gates.shape, F32),
             pltpu.VMEM(sums.shape, F32),
-            pltpu.VMEM((OWNERS, 3, POOLED, HEAD_DIM), BF16),
+            pltpu.VMEM((OWNERS, 2 * POOLED + 16, HEAD_DIM), BF16),
             pltpu.VMEM((n_pool, HEAD_DIM), BF16),
             pltpu.VMEM((n_pool, HEAD_DIM), BF16),
-            pltpu.VMEM((3, POOLED, HEAD_DIM), BF16),
+            pltpu.VMEM((2 * POOLED + 16, HEAD_DIM), BF16),
             pltpu.SemaphoreType.DMA((OWNERS - 1,)),
             pltpu.SemaphoreType.DMA((OWNERS - 1,)),
             pltpu.SemaphoreType.DMA((GATHER_COPIES,)),
@@ -657,15 +657,15 @@
 
         lax.fori_loop(0, SIDE, one, 0)
 
-    lax.fori_loop(0, BLOCKS, attend(0), 0)
+    lax.fori_loop(0, BLOCKS, attend(0), 0, unroll=2)
     product(0)
     meet(len(peers))
     w0.begin()
     w1.begin()
-    lax.fori_loop(0, BLOCKS // 2, attend(1), 0)
+    lax.fori_loop(0, BLOCKS // 2, attend(1), 0, unroll=2)
     w0.combine()
     w1.combine()
-    lax.fori_loop(BLOCKS // 2, BLOCKS, attend(1), 0)
+    lax.fori_loop(BLOCKS // 2, BLOCKS, attend(1), 0, unroll=2)
 
     product(1)
     w2.begin()
@@ -720,24 +720,24 @@
                 at = part * HALF_BLOCK + n * (HALF_BLOCK // 2) + i
                 into[pl.ds(at, POOLED, stride=KEY_BLOCK), :] = rows[i * POOLED : (i + 1) * POOLED]
 
-    weight(0, w0)
-    weight(1, w1)
     k0.combine()
     v0.combine()
     w2.combine2()
     w3.combine2()
     k1.combine()
     v1.combine()
-    weight(2, w2)
-    weight(3, w3)
     k0.turn()
     v0.turn()
     k1.turn()
     v1.turn()
+    weight(0, w0)
+    weight(1, w1)
     k0.combine2()
     v0.combine2()
     k1.combine2()
     v1.combine2()
+    weight(2, w2)
+    weight(3, w3)
     ordered(dk_set, 0, k0)
     ordered(dv_set, 0, v0)
     ordered(dk_set, 1, k1)
@@ -795,18 +795,21 @@
 
 
 def finish_kernel(*refs):
-    for src, out in zip(refs[:4], refs[4:]):
-        out[...] = src[...]
+    copies = [pltpu.make_async_copy(refs[i], refs[4 + i], refs[8].at[i]) for i in range(4)]
+    for copy in copies:
+        copy.start()
+    for copy in copies:
+        copy.wait()
 
 
 def run_finish(*outs):
-    vmem = pl.BlockSpec(memory_space=pltpu.VMEM)
     return pl.pallas_call(
         finish_kernel,
         name="finish",
         out_shape=tuple(jax.ShapeDtypeStruct(a.shape, a.dtype) for a in outs),
-        in_specs=[vmem] * 4,
-        out_specs=(vmem,) * 4,
+        in_specs=[pl.BlockSpec(memory_space=pltpu.VMEM)] * 4,
+        out_specs=(pl.BlockSpec(memory_space=pltpu.HBM),) * 4,
+        scratch_shapes=[pltpu.SemaphoreType.DMA((4,))],
         compiler_params=pltpu.CompilerParams(vmem_limit_bytes=8 * MIB),
     )(*outs)
 

time: 131 us -> 130 us (level)
  no operation moved by 1% of the time
where the time goes in v6:
time: 130 us
  Pallas kernels  129 us (99%)
    pallas_call x1, Pallas kernels, run_scatter(): pl.pallas_call(scatter_kernel, name='scatter', out_shape=(jax.ShapeDtypeS...  70.1 us
    pallas_call x1, Pallas kernels, run_gather(): pl.pallas_call(gather_kernel, name='gather', out_shape=(jax.ShapeDtypeStr...  58 us

profile of v6, /device:TPU:0, one launch (start us, length us, event | category | flops | bytes accessed | tf_op | source)
XLA Modules:
  0.0 130.1 jit_solution(3376299343141673979)
XLA Ops:
  0.6 0.0 copy-start
  0.6 58.0 %gather.1 = (bf16[16,1024,128]{2,1,0:T(8,128)(2,1)S(1)}, bf16[16,1024,128]{2,1,0:T(8,128)(2,1)S(1)}, bf16[8,128,4096]{2,1,0:T(8,128)(2,1)S(1)}, f32[8,128,512]{2...) custom-call(bf16[1024,128]{1,0:T(8,128)(2,1)} %k_ref.1, ...), custom_call_target="tpu_custom_call" | custom-call | flops 40000000000 | bytes 8388608 | tf_op jit(solution)/shard_map/gather/pallas_call | solution.py:341
  58.6 0.0 copy-done
  58.6 70.1 %scatter.1 = (bf16[1024,512]{1,0:T(8,128)(2,1)S(1)}, bf16[1024,128]{1,0:T(8,128)(2,1)S(1)}, bf16[1024,128]{1,0:T(8,128)(2,1)S(1)}, f32[256,512]{1,0:T(8,128)S(1)}) custom-call(s32[8,16]{1,0:T(8,128)S(1)} %bitcast.8, bf16[512,32,128]{2,1,0:T(8,128)(2,1)S(1)} %bitcast.5, bf16[512,32,128]{2,1,0:T(8,128)(2,1)S(1)} %bitcast.6, bf16[1024,4096]{1,0:T(8,128)(2,1)S(1)} %bitcast.4, ...), custom_call_target="tpu_custom_call" | custom-call | tf_op jit(solution)/shard_map/scatter/pallas_call | solution.py:761
  128.7 1.3 %finish.1 = (bf16[1024,512]{1,0:T(8,128)(2,1)}, bf16[1024,128]{1,0:T(8,128)(2,1)}, bf16[1024,128]{1,0:T(8,128)(2,1)}, f32[256,512]{1,0:T(8,128)}) custom-call(bf16[1024,512]{1,0:T(8,128)(2,1)S(1)} %get-tuple-element.30.refs_0_, bf16[1024,128]{1,0:T(8,128)(2,1)S(1)} %get-tuple-element.31.refs_1_, bf16[1024,128]{1,0:T(8,128)(2,1)S(1)} %get-tuple-element.32.refs_2_, ...), custom_call_target="tpu_custom_call" | custom-call | tf_op jit(solution)/shard_map/finish/pallas_call | solution.py:806
Async XLA Ops:
  0.6 58.0 %copy-start = (s32[1,8,16]{2,1,0:T(8,128)S(1)}, s32[1,8,16]{2,1,0:T(8,128)}, u32[]{:S(2)}) copy-start(s32[1,8,16]{2,1,0:T(8,128)} %param.14) | copy-start | bytes 1540

commit v7 on v6

--- a/solution.py
+++ b/solution.py
@@ -112,8 +112,8 @@
 def gather_kernel(
     k_ref, v_ref, h_ref, q_hbm, g_hbm, gate_hbm, ls_hbm, chosen_hbm,
     k_all, v_all, h_all, dq_ref, dpk_ref, dpv_ref, qs_all, cs_all, ls_rows, pick_ref, place_ref,
-    chosen_ref, q_ref, g_ref, gate_ref, ls_ref, pool_all, pk_ref, pv_ref, pool_here,
-    pool_send, pool_recv, send_sems, recv_sems, local_sems,
+    chosen_ref, q_ref, g_ref, gate_ref, ls_ref, pool_k, pool_v, pk_ref, pv_ref,
+    send_sems, recv_sems, local_sems,
 ):
     kv, tp, cz, cy, cx, core = place()
     half = TOKENS // 2
@@ -131,8 +131,7 @@
     def xdev(o, c):
         return (kv, shifted(cx, o) * 2 + c)
 
-    others = [(oz, oy) for oz in range(SIDE) for oy in range(SIDE) if (oz, oy) != (0, 0)]
-    peers = [device(oz, oy) for oz, oy in others] + [
+    peers = [along(axis, s) for axis in (0, 1) for s in (1, -1)] + [
         xdev(1, core), xdev(-1, core), xdev(0, 1 - core)
     ]
     greet(peers)
@@ -158,9 +157,9 @@
     row = lax.broadcasted_iota(jnp.int32, (POOLED, TOKENS), 1)
     mean = jnp.where(row // POOL_BLOCK == blk, 1.0 / POOL_BLOCK, 0.0).astype(BF16)
     local[0].wait()
-    pool_here[:POOLED] = dot(mean, k_all[kv], NN).astype(BF16)
+    pool_k[cz, cy, :POOLED] = dot(mean, k_all[kv], NN).astype(BF16)
     local[1].wait()
-    pool_here[POOLED : POOLED * 2] = dot(mean, v_all[kv], NN).astype(BF16)
+    pool_v[cz, cy] = dot(mean, v_all[kv], NN).astype(BF16)
 
     local[3].wait()
     lane = lax.broadcasted_iota(jnp.int32, (1, LISTED), 1)
@@ -170,16 +169,22 @@
             listed = jnp.where(lane == b * CHOSEN + c, chosen_ref[b, c], listed)
     row = lax.broadcasted_iota(jnp.int32, (16, LISTED), 0)
     both = jnp.where(row == 0, listed // POOLED, jnp.where(row == 1, listed % POOLED, 0))
-    pool_here[POOLED * 2 :] = both.astype(F32).astype(BF16)
+    pool_k[cz, cy, POOLED:] = both.astype(F32).astype(BF16)
     meet(len(peers))
 
-    pool_sender = Sender(pool_send, pool_recv)
-    for oz, oy in others:
-        pool_sender(pool_here, pool_all.at[kv], device(oz, oy))
-    pool_all[kv] = pool_here[...]
-
     send = Sender(send_sems, recv_sems)
-    first, wide = {}, {}
+    first, wide, small = {}, {}, {}
+    pools = ((0, pool_k), (1, pool_v))
+
+    def pool_chunk(axis, ref, o):
+        return ref.at[shifted(cz, o), cy] if axis == 0 else ref.at[cz, shifted(cy, o)]
+
+    def pool_row(axis, ref, o, part=pl.ds(0, SIDE)):
+        return ref.at[part, shifted(cy, o)] if axis == 0 else ref.at[shifted(cz, o), part]
+
+    for axis, ref in pools:
+        here = pool_chunk(axis, ref, 0)
+        small[axis] = [send(here, here, along(axis, s)) for s in (1, -1)]
     arrays = ((0, k_all), (1, v_all))
     for axis, full in arrays:
         here = full.at[kv]
@@ -188,21 +193,74 @@
     here = h_all.at[tp]
     x_first = [send(here, here, xdev(s, core)) for s in (1, -1)]
     x_over = [send(here, here, xdev(0, 1 - core))]
+    for axis, ref in pools:
+        for copy in small[axis]:
+            copy.wait_recv()
+        passed = pool_chunk(axis, ref, -1)
+        small[axis] = [send(passed, passed, along(axis, 1))]
     for axis, full in arrays:
         here = full.at[kv]
         wide[axis] = [(0, [send(here, here, along(1 - axis, s)) for s in (1, -1)])]
+    for axis, ref in pools:
+        small[axis][0].wait_recv()
+        row = pool_row(axis, ref, 0)
+        small[axis] = [send(row, row, along(1 - axis, s)) for s in (1, -1)]
+
+    second = {}
+    for axis, full in arrays:
+        plus, minus = first[axis]
+        plus.wait_recv()
+        part = full.at[owner(axis, -1, 0), pl.ds(0, half)]
+        fwd = send(part, part, along(axis, 1))
+        whole = full.at[owner(axis, -1, 0)]
+        wide[axis].append((-1, [send(whole, whole, along(1 - axis, s)) for s in (1, -1)]))
+        minus.wait_recv()
+        part = full.at[owner(axis, 1, 0), pl.ds(half, half)]
+        bwd = send(part, part, along(axis, -1))
+        second[axis] = (fwd, bwd)
+    for axis, ref in pools:
+        plus, minus = small[axis]
+        plus.wait_recv()
+        part = pool_row(axis, ref, -1, pl.ds(0, 2))
+        minus_part = pool_row(axis, ref, 1, pl.ds(2, 2))
+        fwd = send(part, part, along(1 - axis, 1))
+        minus.wait_recv()
+        small[axis] = [fwd, send(minus_part, minus_part, along(1 - axis, -1))]
+    for axis, full in arrays:
+        whole = full.at[owner(axis, 1, 0)]
+        wide[axis].append((1, [send(whole, whole, along(1 - axis, s)) for s in (1, -1)]))
+
+    last = []
+
+    def across(axis, full, o, pair):
+        plus, minus = pair
+        plus.wait_recv()
+        part = full.at[owner(axis, o, -1), pl.ds(0, half)]
+        last.append(send(part, part, along(1 - axis, 1)))
+        minus.wait_recv()
+        part = full.at[owner(axis, o, 1), pl.ds(half, half)]
+        last.append(send(part, part, along(1 - axis, -1)))
+
+    for axis, full in arrays:
+        across(axis, full, *wide[axis][0])
+    for axis, full in arrays:
+        for copy in second[axis]:
+            copy.wait_recv()
+        whole = full.at[owner(axis, 2, 0)]
+        wide[axis].append((2, [send(whole, whole, along(1 - axis, s)) for s in (1, -1)]))
 
     for copy in local[4:]:
         copy.wait()
-    for copy in pool_sender.sent:
-        copy.wait_recv()
-    pk_ref[...] = pool_all[:, :POOLED].reshape(OWNERS * POOLED, HEAD_DIM)
-    pv_ref[...] = pool_all[:, POOLED : 2 * POOLED].reshape(OWNERS * POOLED, HEAD_DIM)
+    for axis, ref in pools:
+        for copy in small[axis]:
+            copy.wait_recv()
+    pk_ref[...] = pool_k[:, :, :POOLED].reshape(OWNERS * POOLED, HEAD_DIM)
+    pv_ref[...] = pool_v[...].reshape(OWNERS * POOLED, HEAD_DIM)
     dpk_ref[...] = jnp.zeros_like(dpk_ref)
     dpv_ref[...] = jnp.zeros_like(dpv_ref)
 
     def listing(i):
-        both = pool_all[i, 2 * POOLED :].astype(F32)
+        both = pool_k[i // SIDE, i % SIDE, POOLED:].astype(F32)
         owners, numbers, column = both[0:1, :], both[1:2, :], both.T[:, 0:1]
         one = lax.broadcasted_iota(jnp.int32, (LISTED, LISTED), 0)
         two = lax.broadcasted_iota(jnp.int32, (LISTED, LISTED), 1)
@@ -262,45 +320,7 @@
         dpv_ref[...] += dv
         return carry
 
-    lax.fori_loop(0, 4, tile, 0)
-
-    second = {}
-    for axis, full in arrays:
-        plus, minus = first[axis]
-        plus.wait_recv()
-        part = full.at[owner(axis, -1, 0), pl.ds(0, half)]
-        fwd = send(part, part, along(axis, 1))
-        whole = full.at[owner(axis, -1, 0)]
-        wide[axis].append((-1, [send(whole, whole, along(1 - axis, s)) for s in (1, -1)]))
-        minus.wait_recv()
-        part = full.at[owner(axis, 1, 0), pl.ds(half, half)]
-        bwd = send(part, part, along(axis, -1))
-        whole = full.at[owner(axis, 1, 0)]
-        wide[axis].append((1, [send(whole, whole, along(1 - axis, s)) for s in (1, -1)]))
-        second[axis] = (fwd, bwd)
-
-    lax.fori_loop(4, BLOCKS, tile, 0)
-    dpk_ref[...] = dpk_ref[...] * (SCALE / POOL_BLOCK)
-    dpv_ref[...] = dpv_ref[...] * (1.0 / POOL_BLOCK)
-
-    last = []
-
-    def across(axis, full, o, pair):
-        plus, minus = pair
-        plus.wait_recv()
-        part = full.at[owner(axis, o, -1), pl.ds(0, half)]
-        last.append(send(part, part, along(1 - axis, 1)))
-        minus.wait_recv()
-        part = full.at[owner(axis, o, 1), pl.ds(half, half)]
-        last.append(send(part, part, along(1 - axis, -1)))
-
-    for axis, full in arrays:
-        across(axis, full, *wide[axis][0])
-    for axis, full in arrays:
-        for copy in second[axis]:
-            copy.wait_recv()
-        whole = full.at[owner(axis, 2, 0)]
-        wide[axis].append((2, [send(whole, whole, along(1 - axis, s)) for s in (1, -1)]))
+    lax.fori_loop(0, BLOCKS // 2, tile, 0)
     rows = TOKENS // 16
     plus, minus = x_first
     plus.wait_recv()
@@ -313,9 +333,13 @@
     part = whole.at[pl.ds(rows, rows)]
     x_second.append(send(part, part, xdev(-1, core)))
     x_over.append(send(whole, whole, xdev(0, 1 - core)))
-    for i in (1, 2):
-        for axis, full in arrays:
-            across(axis, full, *wide[axis][i])
+    for axis, full in arrays:
+        across(axis, full, *wide[axis][1])
+    lax.fori_loop(BLOCKS // 2, BLOCKS, tile, 0)
+    dpk_ref[...] = dpk_ref[...] * (SCALE / POOL_BLOCK)
+    dpv_ref[...] = dpv_ref[...] * (1.0 / POOL_BLOCK)
+    for axis, full in arrays:
+        across(axis, full, *wide[axis][2])
     for copy in x_second:
         copy.wait_recv()
     whole = h_all.at[shifted(cx, 2) * 2 + core]
@@ -326,11 +350,10 @@
         copy.wait_recv()
     for copy in x_over:
         copy.wait_recv()
-    pool_sender.finish()
     send.finish()
 
 
-GATHER_COPIES = 2 * (2 + 2 + 8 + 8) + 2 + 2 + 4
+GATHER_COPIES = 2 * (2 + 2 + 8 + 8) + 2 + 2 + 4 + 14
 
 
 def run_gather(k, v, h, q, g, gates, sums, chosen):
@@ -362,12 +385,10 @@
             pltpu.VMEM(g.shape, BF16),
             pltpu.VMEM(gates.shape, F32),
             pltpu.VMEM(sums.shape, F32),
-            pltpu.VMEM((OWNERS, 2 * POOLED + 16, HEAD_DIM), BF16),
+            pltpu.VMEM((SIDE, SIDE, POOLED + 16, HEAD_DIM), BF16),
+            pltpu.VMEM((SIDE, SIDE, POOLED, HEAD_DIM), BF16),
             pltpu.VMEM((n_pool, HEAD_DIM), BF16),
             pltpu.VMEM((n_pool, HEAD_DIM), BF16),
-            pltpu.VMEM((2 * POOLED + 16, HEAD_DIM), BF16),
-            pltpu.SemaphoreType.DMA((OWNERS - 1,)),
-            pltpu.SemaphoreType.DMA((OWNERS - 1,)),
             pltpu.SemaphoreType.DMA((GATHER_COPIES,)),
             pltpu.SemaphoreType.DMA((GATHER_COPIES,)),
             pltpu.SemaphoreType.DMA((8,)),

time: 130 us -> 127 us (0.977)
  Pallas kernels: 129 us -> 126 us
    pallas_call x1, Pallas kernels: 58 us -> 55.1 us  [run_gather(): pl.pallas_call(gather_kernel, name='gather', out_shape=(jax.ShapeDtypeStr...]
where the time goes in v7:
time: 127 us
  Pallas kernels  126 us (99%)
    pallas_call x1, Pallas kernels, run_scatter(): pl.pallas_call(scatter_kernel, name='scatter', out_shape=(jax.ShapeDtypeS...  69.9 us
    pallas_call x1, Pallas kernels, run_gather(): pl.pallas_call(gather_kernel, name='gather', out_shape=(jax.ShapeDtypeStr...  55.1 us

profile of v7, /device:TPU:0, one launch (start us, length us, event | category | flops | bytes accessed | tf_op | source)
XLA Modules:
  0.0 127.0 jit_solution(6479476804801292737)
XLA Ops:
  0.6 0.0 copy-start
  0.6 55.1 %gather.1 = (bf16[16,1024,128]{2,1,0:T(8,128)(2,1)S(1)}, bf16[16,1024,128]{2,1,0:T(8,128)(2,1)S(1)}, bf16[8,128,4096]{2,1,0:T(8,128)(2,1)S(1)}, f32[8,128,512]{2...) custom-call(bf16[1024,128]{1,0:T(8,128)(2,1)} %k_ref.1, ...), custom_call_target="tpu_custom_call" | custom-call | flops 40000000000 | bytes 8388608 | tf_op jit(solution)/shard_map/gather/pallas_call | solution.py:364
  55.7 0.0 copy-done
  55.8 69.9 %scatter.1 = (bf16[1024,512]{1,0:T(8,128)(2,1)S(1)}, bf16[1024,128]{1,0:T(8,128)(2,1)S(1)}, bf16[1024,128]{1,0:T(8,128)(2,1)S(1)}, f32[256,512]{1,0:T(8,128)S(1)}) custom-call(s32[8,16]{1,0:T(8,128)S(1)} %bitcast.8, bf16[512,32,128]{2,1,0:T(8,128)(2,1)S(1)} %bitcast.5, bf16[512,32,128]{2,1,0:T(8,128)(2,1)S(1)} %bitcast.6, bf16[1024,4096]{1,0:T(8,128)(2,1)S(1)} %bitcast.4, ...), custom_call_target="tpu_custom_call" | custom-call | tf_op jit(solution)/shard_map/scatter/pallas_call | solution.py:782
  125.6 1.3 %finish.1 = (bf16[1024,512]{1,0:T(8,128)(2,1)}, bf16[1024,128]{1,0:T(8,128)(2,1)}, bf16[1024,128]{1,0:T(8,128)(2,1)}, f32[256,512]{1,0:T(8,128)}) custom-call(bf16[1024,512]{1,0:T(8,128)(2,1)S(1)} %get-tuple-element.30.refs_0_, bf16[1024,128]{1,0:T(8,128)(2,1)S(1)} %get-tuple-element.31.refs_1_, bf16[1024,128]{1,0:T(8,128)(2,1)S(1)} %get-tuple-element.32.refs_2_, ...), custom_call_target="tpu_custom_call" | custom-call | tf_op jit(solution)/shard_map/finish/pallas_call | solution.py:827
Async XLA Ops:
  0.6 55.1 %copy-start = (s32[1,8,16]{2,1,0:T(8,128)S(1)}, s32[1,8,16]{2,1,0:T(8,128)}, u32[]{:S(2)}) copy-start(s32[1,8,16]{2,1,0:T(8,128)} %param.14) | copy-start | bytes 1540

commit v8 on v7

--- a/solution.py
+++ b/solution.py
@@ -106,7 +106,7 @@
     dp = dot(values, cs, NT)
     delta = jnp.sum(p * dp, axis=0, keepdims=True)
     ds = (p * (dp - delta)).astype(BF16)
-    return dot(keys.T, ds, NN), dot(ds, qs, NN), dot(pr, cs, NN)
+    return dot(keys.T, ds, NN), ds, pr
 
 
 def gather_kernel(
@@ -314,10 +314,10 @@
         cs_all[t] = cs[1]
         ls_rows[t] = ls[1]
         visible = ahead <= kv * TOKENS + t * QUERY_BLOCK
-        dq, dk, dv = attend_back(qs, cs[0], ls[0], pk_ref[...], pv_ref[...], visible)
+        dq, ds, pr = attend_back(qs, cs[0], ls[0], pk_ref[...], pv_ref[...], visible)
         dq_ref[t] = dq
-        dpk_ref[...] += dk
-        dpv_ref[...] += dv
+        dpk_ref[...] += dot(ds, qs, NN)
+        dpv_ref[...] += dot(pr, cs[0], NN)
         return carry
 
     lax.fori_loop(0, BLOCKS // 2, tile, 0)
@@ -593,7 +593,7 @@
 def scatter_kernel(
     chosen_ref, k_ref, v_ref, h_ref, dqp_ref, dpk_ref, dpv_ref, qs_all, cs_all, ls_rows, pick_ref, place_ref,
     gq_ref, gk_out, gv_out, gw_out,
-    kb, vb, dk_set, dv_set, gqt, dk0, dv0, dk1, dv1, own_k, own_v, gw0, gw1, gw2, gw3, *rest
+    kb, vb, ds_held, pr_held, dk_set, dv_set, gqt, dk0, dv0, dk1, dv1, own_k, own_v, gw0, gw1, gw2, gw3, *rest
 ):
     cut = 4 * LISTED_BUFS
     bufs = [rest[i * LISTED_BUFS : (i + 1) * LISTED_BUFS] for i in range(4)]
@@ -639,7 +639,7 @@
                 kb[c * KEY_BLOCK : (c + 1) * KEY_BLOCK, :] = k_ref[at]
                 vb[c * KEY_BLOCK : (c + 1) * KEY_BLOCK, :] = v_ref[at]
                 seen.append(ahead <= start_row - at * KEY_BLOCK)
-            dq, dk, dv = attend_back(
+            dq, ds, pr = attend_back(
                 qs_all[b, across, :],
                 cs_all[b, across, :],
                 ls_rows[b, :, across],
@@ -654,16 +654,30 @@
                 at = pair * PAIR + h * HEAD_DIM
                 gqt[at : at + HEAD_DIM, rows] = part.astype(BF16)
                 gq_ref[rows, at : at + HEAD_DIM] = part.T.astype(BF16)
-            here = pl.ds(pl.multiple_of(b * SETS, SETS), SETS)
             if pair == 0:
-                dk_set[here, :] = dk * SCALE
-                dv_set[here, :] = dv
+                ds_held[b] = ds
+                pr_held[b] = pr
             else:
-                dk_set[here, :] += dk * SCALE
-                dv_set[here, :] += dv
+                for i in (0, 1):
+                    at, rows = 2 * b + i, slice(i * PAIR_Q, (i + 1) * PAIR_Q)
+                    spot = (at // SIDE, at % SIDE, slice(0, PAIR_Q))
+                    dk0[spot], dk1[spot] = ds[rows, :HEAD_DIM], ds[rows, HEAD_DIM:]
+                    dv0[spot], dv1[spot] = pr[rows, :HEAD_DIM], pr[rows, HEAD_DIM:]
             return carry
 
         return block
+
+    def sets(b, carry):
+        here = pl.ds(pl.multiple_of(b * SETS, SETS), SETS)
+
+        def whole(held, low, high):
+            at = [((2 * b + i) // SIDE, (2 * b + i) % SIDE, slice(0, PAIR_Q)) for i in (0, 1)]
+            parts = [jnp.concatenate([ref[a] for a in at], axis=0) for ref in (low, high)]
+            return jnp.concatenate([held[b], *parts], axis=1)
+
+        dk_set[here, :] = dot(whole(ds_held, dk0, dk1), qs_all[b], NN) * SCALE
+        dv_set[here, :] = dot(whole(pr_held, dv0, dv1), cs_all[b], NN)
+        return carry
 
     def product(pair):
         def one(j, carry):
@@ -691,6 +705,7 @@
     product(1)
     w2.begin()
     w3.begin()
+    lax.fori_loop(0, BLOCKS, sets, 0, unroll=2)
     w0.turn()
     w1.turn()
 
@@ -769,7 +784,7 @@
 
 
 SCATTER_COPIES = 8 * 12
-SCATTER_MIB = 28
+SCATTER_MIB = 31.2
 
 
 def run_scatter(chosen, k_all, v_all, h_all, dqp, dpk, dpv, qs, cs, ls, pick, places):
@@ -793,6 +808,8 @@
         scratch_shapes=[
             pltpu.VMEM((SETS, HEAD_DIM), BF16),
             pltpu.VMEM((SETS, HEAD_DIM), BF16),
+            pltpu.VMEM((BLOCKS, SETS, PAIR_Q), BF16),
+            pltpu.VMEM((BLOCKS, SETS, PAIR_Q), BF16),
             pltpu.VMEM((BLOCKS * SETS, HEAD_DIM), F32),
             pltpu.VMEM((BLOCKS * SETS, HEAD_DIM), F32),
             pltpu.VMEM((GROUP * HEAD_DIM, TOKENS), BF16),
@@ -810,7 +827,7 @@
             pltpu.SemaphoreType.DMA((SCATTER_COPIES,)),
         ],
         compiler_params=pltpu.CompilerParams(
-            collective_id=1, has_side_effects=True, vmem_limit_bytes=SCATTER_MIB * MIB
+            collective_id=1, has_side_effects=True, vmem_limit_bytes=int(SCATTER_MIB * MIB)
         ),
     )(chosen, k_all, v_all, h_all, dqp, dpk, dpv, qs, cs, ls, pick, places)
 

time: 127 us -> 125 us (0.984)
  Pallas kernels: 126 us -> 124 us
    pallas_call x1, Pallas kernels: 69.9 us -> 67.8 us  [run_scatter(): pl.pallas_call(scatter_kernel, name='scatter', out_shape=(jax.ShapeDtypeS...]
where the time goes in v8:
time: 125 us
  Pallas kernels  124 us (99%)
    pallas_call x1, Pallas kernels, run_scatter(): pl.pallas_call(scatter_kernel, name='scatter', out_shape=(jax.ShapeDtypeS...  67.8 us
    pallas_call x1, Pallas kernels, run_gather(): pl.pallas_call(gather_kernel, name='gather', out_shape=(jax.ShapeDtypeStr...  55.1 us

profile of v8, /device:TPU:0, one launch (start us, length us, event | category | flops | bytes accessed | tf_op | source)
XLA Modules:
  0.0 124.9 jit_solution(13762961514995786711)
XLA Ops:
  0.6 0.0 copy-start
  0.6 55.1 %gather.1 = (bf16[16,1024,128]{2,1,0:T(8,128)(2,1)S(1)}, bf16[16,1024,128]{2,1,0:T(8,128)(2,1)S(1)}, bf16[8,128,4096]{2,1,0:T(8,128)(2,1)S(1)}, f32[8,128,512]{2...) custom-call(bf16[1024,128]{1,0:T(8,128)(2,1)} %k_ref.1, ...), custom_call_target="tpu_custom_call" | custom-call | flops 40000000000 | bytes 8388608 | tf_op jit(solution)/shard_map/gather/pallas_call | solution.py:364
  55.7 0.0 copy-done
  55.7 67.8 %scatter.1 = (bf16[1024,512]{1,0:T(8,128)(2,1)S(1)}, bf16[1024,128]{1,0:T(8,128)(2,1)S(1)}, bf16[1024,128]{1,0:T(8,128)(2,1)S(1)}, f32[256,512]{1,0:T(8,128)S(1)}) custom-call(s32[8,16]{1,0:T(8,128)S(1)} %bitcast.8, bf16[512,32,128]{2,1,0:T(8,128)(2,1)S(1)} %bitcast.5, bf16[512,32,128]{2,1,0:T(8,128)(2,1)S(1)} %bitcast.6, bf16[1024,4096]{1,0:T(8,128)(2,1)S(1)} %bitcast.4, ...), custom_call_target="tpu_custom_call" | custom-call | tf_op jit(solution)/shard_map/scatter/pallas_call | solution.py:797
  123.5 1.3 %finish.1 = (bf16[1024,512]{1,0:T(8,128)(2,1)}, bf16[1024,128]{1,0:T(8,128)(2,1)}, bf16[1024,128]{1,0:T(8,128)(2,1)}, f32[256,512]{1,0:T(8,128)}) custom-call(bf16[1024,512]{1,0:T(8,128)(2,1)S(1)} %get-tuple-element.30.refs_0_, bf16[1024,128]{1,0:T(8,128)(2,1)S(1)} %get-tuple-element.31.refs_1_, bf16[1024,128]{1,0:T(8,128)(2,1)S(1)} %get-tuple-element.32.refs_2_, ...), custom_call_target="tpu_custom_call" | custom-call | tf_op jit(solution)/shard_map/finish/pallas_call | solution.py:844
Async XLA Ops:
  0.6 55.1 %copy-start = (s32[1,8,16]{2,1,0:T(8,128)S(1)}, s32[1,8,16]{2,1,0:T(8,128)}, u32[]{:S(2)}) copy-start(s32[1,8,16]{2,1,0:T(8,128)} %param.14) | copy-start | bytes 1540

commit v9 on v8

--- a/solution.py
+++ b/solution.py
@@ -766,12 +766,12 @@
     v0.turn()
     k1.turn()
     v1.turn()
-    weight(0, w0)
-    weight(1, w1)
     k0.combine2()
     v0.combine2()
     k1.combine2()
     v1.combine2()
+    weight(0, w0)
+    weight(1, w1)
     weight(2, w2)
     weight(3, w3)
     ordered(dk_set, 0, k0)

time: 125 us -> 125 us (level)
  no operation moved by 1% of the time
where the time goes in v9:
time: 125 us
  Pallas kernels  124 us (99%)
    pallas_call x1, Pallas kernels, run_scatter(): pl.pallas_call(scatter_kernel, name='scatter', out_shape=(jax.ShapeDtypeS...  67.7 us
    pallas_call x1, Pallas kernels, run_gather(): pl.pallas_call(gather_kernel, name='gather', out_shape=(jax.ShapeDtypeStr...  55.1 us

profile of v9, /device:TPU:0, one launch (start us, length us, event | category | flops | bytes accessed | tf_op | source)
XLA Modules:
  0.0 124.8 jit_solution(3748825029841012765)
XLA Ops:
  0.6 0.0 copy-start
  0.6 55.1 %gather.1 = (bf16[16,1024,128]{2,1,0:T(8,128)(2,1)S(1)}, bf16[16,1024,128]{2,1,0:T(8,128)(2,1)S(1)}, bf16[8,128,4096]{2,1,0:T(8,128)(2,1)S(1)}, f32[8,128,512]{2...) custom-call(bf16[1024,128]{1,0:T(8,128)(2,1)} %k_ref.1, ...), custom_call_target="tpu_custom_call" | custom-call | flops 40000000000 | bytes 8388608 | tf_op jit(solution)/shard_map/gather/pallas_call | solution.py:364
  55.7 0.0 copy-done
  55.7 67.7 %scatter.1 = (bf16[1024,512]{1,0:T(8,128)(2,1)S(1)}, bf16[1024,128]{1,0:T(8,128)(2,1)S(1)}, bf16[1024,128]{1,0:T(8,128)(2,1)S(1)}, f32[256,512]{1,0:T(8,128)S(1)}) custom-call(s32[8,16]{1,0:T(8,128)S(1)} %bitcast.8, bf16[512,32,128]{2,1,0:T(8,128)(2,1)S(1)} %bitcast.5, bf16[512,32,128]{2,1,0:T(8,128)(2,1)S(1)} %bitcast.6, bf16[1024,4096]{1,0:T(8,128)(2,1)S(1)} %bitcast.4, ...), custom_call_target="tpu_custom_call" | custom-call | tf_op jit(solution)/shard_map/scatter/pallas_call | solution.py:797
  123.5 1.3 %finish.1 = (bf16[1024,512]{1,0:T(8,128)(2,1)}, bf16[1024,128]{1,0:T(8,128)(2,1)}, bf16[1024,128]{1,0:T(8,128)(2,1)}, f32[256,512]{1,0:T(8,128)}) custom-call(bf16[1024,512]{1,0:T(8,128)(2,1)S(1)} %get-tuple-element.30.refs_0_, bf16[1024,128]{1,0:T(8,128)(2,1)S(1)} %get-tuple-element.31.refs_1_, bf16[1024,128]{1,0:T(8,128)(2,1)S(1)} %get-tuple-element.32.refs_2_, ...), custom_call_target="tpu_custom_call" | custom-call | tf_op jit(solution)/shard_map/finish/pallas_call | solution.py:844
Async XLA Ops:
  0.6 55.1 %copy-start = (s32[1,8,16]{2,1,0:T(8,128)S(1)}, s32[1,8,16]{2,1,0:T(8,128)}, u32[]{:S(2)}) copy-start(s32[1,8,16]{2,1,0:T(8,128)} %param.14) | copy-start | bytes 1540
